TPU v7x, 32 devices: a whole 2x2x4 slice. The times are simulated.
32 devices in a mesh: ep: 8 (over z, x), tp: 4 (over y, core).
Axes of the slice: x: 2, y: 2, z: 4, core: 2. Of those that a mesh axis runs over, the one named last changes fastest.
Arguments:
- tokens: bfloat16 [512, 4096], P('ep'), may hold values from -6 to 6
- state_in: float32 [512, 4096], P('ep', 'tp'), may hold values from -6 to 6
- conv_in: bfloat16 [512, 3, 4096], P('ep', None, 'tp'), may hold values from -6 to 6
- mix_gain: bfloat16 [4096], replicated, may hold values from 0.099609375 to 1.8984375
- rnn_weight: bfloat16 [4096, 4096], P('ep', 'tp'), may hold values from -0.09375 to 0.09375
- gate_weight: bfloat16 [4096, 4096], P('ep', 'tp'), may hold values from -0.09375 to 0.09375
- conv_weight: bfloat16 [4, 4096], P(None, 'tp'), may hold values from -3 to 3
- rate_weight: bfloat16 [16, 256, 256], P('tp'), may hold values from -0.375 to 0.375
- input_weight: bfloat16 [16, 256, 256], P('tp'), may hold values from -0.375 to 0.375
- rate_param: float32 [4096], P('tp'), may hold values from 1 to 6
- out_weight: bfloat16 [4096, 4096], P('tp'), may hold values from -0.09375 to 0.09375
- moe_gain: bfloat16 [4096], replicated, may hold values from 0.099609375 to 1.8984375
- expert_gate: bfloat16 [8, 4096, 2048], P('ep', None, 'tp'), may hold values from -0.09375 to 0.09375
- expert_up: bfloat16 [8, 4096, 2048], P('ep', None, 'tp'), may hold values from -0.09375 to 0.09375
- expert_down: bfloat16 [8, 2048, 4096], P('ep', 'tp'), may hold values from -0.125 to 0.125
- routes: int32 [512, 2], P('ep'), may hold values from 0 to 7, all different within a row; in each aligned block of 64 rows (0 to 63, 64 to 127, ...) at most 32 rows name the same one
- route_prob: float32 [512, 2], P('ep'), may hold values from 0.1 to 1
Outputs:
- layer_out: bfloat16 [512, 4096], P('ep', 'tp')
- state_out: float32 [512, 4096], P('ep', 'tp')
- conv_out: bfloat16 [512, 3, 4096], P('ep', None, 'tp')
Inputs may be any that keep to these rules, and one draw needn't show every extreme that they name: `routes`: the 2 experts of a sequence differ. Among the rows of one index of ep no expert is named more than 32 times, and in every draw some expert is named exactly 32 times there.
All inputs are finite; a program needn't handle non-finite values.
Results may differ from a plain program's by a relative error of at most 0.014.
Values may be sent and summed in bfloat16 or wider, within the bound.
No kernel may reach another device: no remote copies, remote signals or barrier semaphores. Data moves between devices by JAX's collectives and lax.ppermute only.
A program may use at most 64 MiB of HBM per device.

v0:
```python
import jax
import jax.numpy as jnp
from jax import lax
from jax.sharding import PartitionSpec as P


def rms_scale(values, gain):
    scale = lax.rsqrt(jnp.mean(values * values, axis=-1, keepdims=True) + 1e-06)
    return values * scale * gain.astype(jnp.float32)


def slot_targets(route_ids, experts, capacity):
    flat_ids = route_ids.reshape(-1)
    onehot = (flat_ids[:, None] == jnp.arange(experts, dtype=jnp.int32)[None, :]).astype(jnp.int32)
    before = jnp.cumsum(onehot, axis=0) - onehot
    slot_ids = jnp.sum(before * onehot, axis=1)
    return flat_ids * capacity + slot_ids


def block_map(conv, weight):
    rows = conv.shape[0]
    blocks = weight.shape[0]
    parts = conv.reshape(rows, blocks, weight.shape[1])
    mapped = jnp.einsum("snc,ncd->snd", parts, weight, preferred_element_type=jnp.float32)
    return mapped.reshape(rows, blocks * weight.shape[2])


def shards(
    tokens,
    state_in,
    conv_in,
    mix_gain,
    rnn_weight,
    gate_weight,
    conv_weight,
    rate_weight,
    input_weight,
    rate_param,
    out_weight,
    moe_gain,
    expert_gate,
    expert_up,
    expert_down,
    routes,
    route_prob,
):
    group_rows = tokens.shape[0]
    model_width = tokens.shape[1]
    channels = rnn_weight.shape[1]
    base = tokens.astype(jnp.float32)
    normed = rms_scale(base, mix_gain).astype(jnp.bfloat16)
    columns = lax.all_to_all(normed, "ep", split_axis=1, concat_axis=0, tiled=True)
    joined = jnp.concatenate([rnn_weight, gate_weight], axis=1)
    summed = lax.psum_scatter(
        jnp.dot(columns, joined, preferred_element_type=jnp.float32).astype(jnp.bfloat16),
        "ep",
        scatter_dimension=0,
        tiled=True,
    ).astype(jnp.float32)
    proj_x = summed[:, :channels]
    proj_y = summed[:, channels:]
    moved = proj_x.astype(jnp.bfloat16)
    conv_out = jnp.concatenate([conv_in[:, 1:], moved[:, None, :]], axis=1)
    taps = conv_weight.astype(jnp.float32)
    history = conv_in.astype(jnp.float32)
    mixed_in = (
        history[:, 0] * taps[0]
        + history[:, 1] * taps[1]
        + history[:, 2] * taps[2]
        + moved.astype(jnp.float32) * taps[3]
    )
    conv = mixed_in.astype(jnp.bfloat16)
    rate = jax.nn.sigmoid(block_map(conv, rate_weight))
    in_gate = jax.nn.sigmoid(block_map(conv, input_weight))
    log_decay = -8.0 * rate * jax.nn.softplus(-rate_param)
    state_out = jnp.exp(log_decay) * state_in + jnp.sqrt(
        -jnp.expm1(2.0 * log_decay)
    ) * in_gate * conv.astype(jnp.float32)
    gated = (state_out * jax.nn.gelu(proj_y, approximate=True)).astype(jnp.bfloat16)
    partial_out = jnp.dot(gated, out_weight, preferred_element_type=jnp.float32)
    mixed = base + lax.psum(partial_out.astype(jnp.bfloat16), "tp").astype(jnp.float32)
    normed2 = rms_scale(mixed, moe_gain).astype(jnp.bfloat16)
    experts = lax.axis_size("ep")
    topk = routes.shape[1]
    capacity = max(2, 2 * group_rows * topk // experts)
    targets = slot_targets(routes, experts, capacity)
    dispatch = (
        jnp.arange(experts * capacity, dtype=jnp.int32)[:, None] == targets[None, :]
    ).astype(jnp.bfloat16)
    repeated = jnp.repeat(normed2, topk, axis=0)
    send = jnp.dot(dispatch, repeated, preferred_element_type=jnp.float32).astype(jnp.bfloat16)
    send = send.reshape(experts, capacity, model_width)
    received = lax.all_to_all(send, "ep", split_axis=0, concat_axis=0, tiled=True)
    flat_rows = received.reshape(-1, model_width)
    gate_part = jnp.dot(flat_rows, expert_gate[0], preferred_element_type=jnp.float32)
    up_part = jnp.dot(flat_rows, expert_up[0], preferred_element_type=jnp.float32)
    hidden = (jax.nn.silu(gate_part) * up_part).astype(jnp.bfloat16)
    result = jnp.dot(hidden, expert_down[0], preferred_element_type=jnp.float32)
    partial_experts = result.reshape(received.shape[0], received.shape[1], model_width)
    reduced = lax.psum_scatter(
        partial_experts.astype(jnp.bfloat16), "tp", scatter_dimension=2, tiled=True
    )
    returned = lax.all_to_all(reduced, "ep", split_axis=0, concat_axis=0, tiled=True)
    share = returned.shape[2]
    picked = jnp.einsum(
        "rj,rd->jd",
        dispatch,
        returned.reshape(experts * capacity, share),
        preferred_element_type=jnp.float32,
    )
    weights = route_prob / jnp.sum(route_prob, axis=1, keepdims=True)
    experts_sum = jnp.sum(picked.reshape(group_rows, topk, share) * weights[:, :, None], axis=1)
    own_columns = lax.dynamic_slice_in_dim(mixed, lax.axis_index("tp") * share, share, 1)
    layer_out = (own_columns + experts_sum).astype(jnp.bfloat16)
    return (layer_out, state_out, conv_out)


def solution(mesh):
    in_specs = (
        P("ep", None),
        P("ep", "tp"),
        P("ep", None, "tp"),
        P(),
        P("ep", "tp"),
        P("ep", "tp"),
        P(None, "tp"),
        P("tp", None, None),
        P("tp", None, None),
        P("tp"),
        P("tp", None),
        P(),
        P("ep", None, "tp"),
        P("ep", None, "tp"),
        P("ep", "tp", None),
        P("ep", None),
        P("ep", None),
    )
    out_specs = (P("ep", "tp"), P("ep", "tp"), P("ep", None, "tp"))
    return jax.shard_map(shards, mesh=mesh, in_specs=in_specs, out_specs=out_specs, check_vma=False)
```

profile of v0, /device:TPU:0, one launch (start us, length us, event | category | flops | bytes accessed | tf_op | source)
XLA Modules:
  0.0 267.9 jit_solution(9502218566155616131)
XLA Ops:
  7.2 0.7 convert_element_type.63
  8.0 1.2 fusion.23
  9.2 1.2 fusion.25
  10.5 21.6 %all_to_all.29 = bf16[64,8,512]{2,0,1:T(8,128)(2,1)S(1)} all-to-all(bf16[64,8,512]{2,0,1:T(8,128)(2,1)S(1)} %bitcast.85), channel_id=1, replica_groups=mesh['ep'=8,'tp'=4] {'ep'}, dimensions={1} | all-to-all | bytes 1048576 | tf_op jit(solution)/shard_map/all_to_all | solution.py:52
  32.1 4.2 %convolution_convert_fusion.3 = bf16[512,2048]{1,0:T(8,128)(2,1)} fusion(bf16[512,512]{1,0:T(8,128)(2,1)S(1)} %bitcast.88, bf16[512,1024]{1,0:T(8,128)(2,1)} %param.22, bf16[512,1024]{1,0:T(8,128)(2,1)} %param.21), kind=kOutput, calls=%fused_computation.8 | convolution fusion | flops 1078984704 | bytes 4718592 | tf_op jit(solution)/shard_map/dot_general | solution.py:55
  37.1 66.8 %reduce-scatter.3.cloned.1.call-done = bf16[64,2048]{1,0:T(8,128)(2,1)} async-done(((bf16[512,2048]{1,0:T(8,128)(2,1)}), bf16[64,2048]{1,0:T(8,128)(2,1)}) %reduce-scatter.3.cloned.1.call-update) | async-done | bytes 262160 | tf_op jit(solution)/shard_map/reduce_scatter | solution.py:54
  103.8 1.1 fusion.36
  105.8 5.9 %convolution_convert_fusion.2 = bf16[64,4096]{1,0:T(8,128)(2,1)} fusion(bf16[1024,4096]{1,0:T(8,128)(2,1)} %param.27, f32[64,1024]{1,0:T(8,128)S(1)} %multiply_add_fusion, bf16[64,2048]{1,0:T(8,128)(2,1)S(1)} %copy-done.4), kind=kOutput, calls=%fused_computation.2 | convolution fusion | flops 537853952 | bytes 9306112 | tf_op jit(solution)/shard_map/dot_general | solution.py:80
  111.9 32.4 %all-reduce.2.cloned.1.call-done = bf16[64,4096]{1,0:T(8,128)(2,1)} async-done(((bf16[64,4096]{1,0:T(8,128)(2,1)}), bf16[64,4096]{1,0:T(8,128)(2,1)}) %all-reduce.2.cloned.1.call-update) | async-done | bytes 524304 | tf_op jit(solution)/shard_map/psum | solution.py:81
  144.3 2.3 convert_add_fusion
  146.6 1.3 multiply_convert_fusion
  147.9 1.0 broadcast_in_dim.4
  149.4 0.7 convolution_convert_fusion
  150.1 52.8 %all_to_all.30 = bf16[8,32,4096]{2,1,0:T(8,128)(2,1)S(1)} all-to-all(bf16[8,32,4096]{2,1,0:T(8,128)(2,1)S(1)} %bitcast.80), channel_id=1, replica_groups=mesh['ep'=8,'tp'=4] {'ep'}, dimensions={0} | all-to-all | bytes 4194304 | tf_op jit(solution)/shard_map/all_to_all | solution.py:93
  202.9 1.2 fusion.3
  204.1 0.9 copy-done.12
  205.1 1.3 fusion.11
  206.3 0.9 copy-done.13
  207.2 2.6 convolution_convert_fusion.1
  209.9 29.8 %reduce-scatter.5.cloned.1.call-done = bf16[8,32,1024]{2,1,0:T(8,128)(2,1)} async-done(((bf16[8,32,4096]{2,1,0:T(8,128)(2,1)}), bf16[8,32,1024]{2,1,0:T(8,128)(2,1)}) %reduce-scatter.5.cloned.1.call-update) | async-done | bytes 524304 | tf_op jit(solution)/shard_map/reduce_scatter | solution.py:100
  239.7 5.5 %all-to-all-start.2 = ((bf16[8,32,1024]{2,1,0:T(8,128)(2,1)}), bf16[8,32,1024]{2,1,0:T(8,128)(2,1)S(1)}, u32[]{:S(2)}, u32[]{:S(2)}) async-start(bf16[8,32,1024]{2,1,0:T(8,128)(2,1)} %reduce-scatter.5.cloned.1.call-done), calls=%async_computation.4 | async-start | bytes 1048576 | tf_op jit(solution)/shard_map/all_to_all | solution.py:103
  245.4 0.8 pad_maximum_fusion
  246.2 13.3 %all-to-all-done.2 = bf16[8,32,1024]{2,1,0:T(8,128)(2,1)S(1)} async-done(((bf16[8,32,1024]{2,1,0:T(8,128)(2,1)}), bf16[8,32,1024]{2,1,0:T(8,128)(2,1)S(1)}, u32[]{:S(2)}, u32[]{:S(2)}) %all-to-all-start.2) | async-done | bytes 524320 | tf_op jit(solution)/shard_map/all_to_all | solution.py:103
  259.7 1.6 add_convert_fusion
  (61 shorter events, 2.7 us)
Async XLA Ops:
  7.2 97.7 %copy-start = (bf16[4,256,256]{2,1,0:T(8,128)(2,1)S(1)}, bf16[4,256,256]{2,1,0:T(8,128)(2,1)}, u32[]{:S(2)}) copy-start(bf16[4,256,256]{2,1,0:T(8,128)(2,1)} %param.24) | copy-start | bytes 1572868
  7.2 96.7 %reduce-scatter.3.cloned.1.call-start = ((), (), s32[]{:S(2)}) async-start(), calls=%async_computation.5 | async-start | bytes 2359296 | tf_op jit(solution)/shard_map/reduce_scatter | solution.py:54
  32.1 4.3 %copy-start.3 = (bf16[64,3,1024]{2,0,1:T(8,128)(2,1)S(1)}, bf16[64,3,1024]{2,0,1:T(8,128)(2,1)}, u32[]{:S(2)}) copy-start(bf16[64,3,1024]{2,0,1:T(8,128)(2,1)} %param.19) | copy-start | bytes 1179652
  32.1 4.4 %copy-start.10 = (s32[64,2]{0,1:T(2,128)S(1)}, s32[64,2]{0,1:T(2,128)}, u32[]{:S(2)}) copy-start(s32[64,2]{0,1:T(2,128)} %param.32) | copy-start | bytes 1540
  32.1 4.9 %copy-start.8 = (f32[1024]{0:T(1024)S(1)}, f32[1024]{0:T(1024)}, u32[]{:S(2)}) copy-start(f32[1024]{0:T(1024)} %param.26) | copy-start | bytes 12292
  32.1 4.9 %copy-start.6 = (bf16[4,1024]{1,0:T(4,128)(2,1)S(1)}, bf16[4,1024]{1,0:T(4,128)(2,1)}, u32[]{:S(2)}) copy-start(bf16[4,1024]{1,0:T(4,128)(2,1)} %param.23) | copy-start | bytes 24580
  36.3 68.9 %copy-start.14 = (bf16[4,256,256]{2,1,0:T(8,128)(2,1)S(1)}, bf16[4,256,256]{2,1,0:T(8,128)(2,1)}, u32[]{:S(2)}) copy-start(bf16[4,256,256]{2,1,0:T(8,128)(2,1)} %param.25) | copy-start | bytes 1572868
  36.3 69.2 %copy-start.5 = (f32[64,1024]{1,0:T(8,128)S(1)}, f32[64,1024]{1,0:T(8,128)}, u32[]{:S(2)}) copy-start(f32[64,1024]{1,0:T(8,128)} %param.18) | copy-start | bytes 786436
  36.4 107.9 %all-reduce.2.cloned.1.call-start = ((), (), s32[]{:S(2)}) async-start(), calls=%async_computation.6 | async-start | bytes 1048576 | tf_op jit(solution)/shard_map/psum | solution.py:81
  103.8 1.9 copy-start.4
  105.7 5.9 %copy-start.2 = (f32[64,1024]{1,0:T(8,128)}, f32[64,1024]{1,0:T(8,128)S(1)}, u32[]{:S(2)}) copy-start(f32[64,1024]{1,0:T(8,128)S(1)} %multiply_add_fusion) | copy-start | bytes 786436
  105.7 6.2 %copy-start.7 = (bf16[4096]{0:T(1024)(128)(2,1)S(1)}, bf16[4096]{0:T(1024)(128)(2,1)}, u32[]{:S(2)}) copy-start(bf16[4096]{0:T(1024)(128)(2,1)} %param.28) | copy-start | bytes 24580
  105.8 38.5 %copy-start.1 = (bf16[64,4096]{1,0:T(8,128)(2,1)S(1)}, bf16[64,4096]{1,0:T(8,128)(2,1)}, u32[]{:S(2)}) copy-start(bf16[64,4096]{1,0:T(8,128)(2,1)} %param.17) | copy-start | bytes 1572868
  111.7 128.0 %reduce-scatter.5.cloned.1.call-start = ((), (), s32[]{:S(2)}) async-start(), calls=%async_computation.7 | async-start | bytes 2621440 | tf_op jit(solution)/shard_map/reduce_scatter | solution.py:100
  149.3 53.5 %copy-start.11 = (bf16[1,4096,512]{2,1,0:T(8,128)(2,1)S(1)}, bf16[1,4096,512]{2,1,0:T(8,128)(2,1)}, u32[]{:S(2)}) copy-start(bf16[1,4096,512]{2,1,0:T(8,128)(2,1)} %param.29) | copy-start | bytes 12582916
  202.9 2.2 copy-start.12
  205.1 2.2 copy-start.13
  207.2 38.1 %copy-start.9 = (f32[64,2]{0,1:T(2,128)S(1)}, f32[64,2]{0,1:T(2,128)}, u32[]{:S(2)}) copy-start(f32[64,2]{0,1:T(2,128)} %param.33) | copy-start | bytes 1540
  207.2 38.1 %slice-start = ((bf16[64,3,1024]{2,0,1:T(8,128)(2,1)}), bf16[64,2,1024]{2,0,1:T(8,128)(2,1)S(1)}, s32[]{:S(2)}) async-start(bf16[64,3,1024]{2,0,1:T(8,128)(2,1)} %param.19), calls=%async_computation.8 | async-start | bytes 524288 | tf_op jit(solution)/shard_map/slice | solution.py:63
  239.7 19.8 %all-to-all-start.2 = ((bf16[8,32,1024]{2,1,0:T(8,128)(2,1)}), bf16[8,32,1024]{2,1,0:T(8,128)(2,1)S(1)}, u32[]{:S(2)}, u32[]{:S(2)}) async-start(bf16[8,32,1024]{2,1,0:T(8,128)(2,1)} %reduce-scatter.5.cloned.1.call-done), calls=%async_computation.4 | async-start | bytes 1048576 | tf_op jit(solution)/shard_map/all_to_all | solution.py:103
Sparse Core Ops, SparseCore 0:
  36.5 67.3 reduce-scatter.2
  111.8 32.4 all-reduce.1
  210.0 29.6 reduce-scatter.4
where the time goes:
time: 269 us; the launch traced here: 268 us
  waiting for transfers between devices  142 us (53%)
  blocking collectives  74.4 us (28%)
  matrix products  16.6 us (6%)
  between operations  14.1 us (5%)
  other arithmetic  11.2 us (4%)
  starting transfers between devices  5.64 us (2%)
  local copies, waits for them, and re-layouts  3.75 us (1%)
    reduce_scatter x1, waiting for transfers between devices, shards(): lax.psum_scatter(jnp.dot(columns, joined, preferred_element_type=jnp.floa...  66.8 us
    all_to_all x1, blocking collectives, shards(): lax.all_to_all(send, 'ep', split_axis=0, concat_axis=0, tiled=True)  52.8 us
    psum x1, waiting for transfers between devices, shards(): lax.psum(partial_out.astype(jnp.bfloat16), 'tp').astype(jnp.float32)  32.4 us
    reduce_scatter x1, waiting for transfers between devices, shards(): lax.psum_scatter(partial_experts.astype(jnp.bfloat16), 'tp', scatter_dime...  29.8 us
    all_to_all x1, blocking collectives, shards(): lax.all_to_all(normed, 'ep', split_axis=1, concat_axis=0, tiled=True)  21.6 us
    all_to_all x1, waiting for transfers between devices, shards(): lax.all_to_all(reduced, 'ep', split_axis=0, concat_axis=0, tiled=True)  13.3 us
    dot_general x1, matrix products, shards(): partial_out = jnp.dot(gated, out_weight, preferred_element_type=jnp.float32)  5.88 us
    all_to_all x1, starting transfers between devices, shards(): lax.all_to_all(reduced, 'ep', split_axis=0, concat_axis=0, tiled=True)  5.51 us
  transfers between devices with their start and end apart: 4, of which 4 were waited for; matrix products, arithmetic and copies ran while one was open for 1% of the time, Pallas kernels for 0%

commit v1 on v0

v1 whole, which is shorter than its diff:
```python
import functools

import jax
import jax.numpy as jnp
from jax import lax
from jax.experimental import pallas as pl
from jax.experimental.pallas import tpu as pltpu
from jax.sharding import PartitionSpec as P


AXES = ("ep", "tp")
CORES = 2


def send_to(value, target):
    n_ep, n_tp = lax.axis_size("ep"), lax.axis_size("tp")
    pairs = []
    for e in range(n_ep):
        for t in range(n_tp):
            to_e, to_t = target(e, t)
            pairs.append((e * n_tp + t, to_e * n_tp + to_t))
    return lax.ppermute(value, AXES, pairs)


def across_ep(value, offset):
    return send_to(value, lambda e, t: (e ^ offset, t))


def across_cores(value):
    return send_to(value, lambda e, t: (e, t ^ 1))


def across_y(value, offset):
    return send_to(value, lambda e, t: (e, t ^ (CORES * offset)))


def halving_sum(blocks, weight, bits):
    order = [0]
    for bit in reversed(bits):
        order = order + [d | (1 << bit) for d in order]
    half = len(order) // 2
    sent_rows = jnp.concatenate([blocks[d] for d in order[half:]], axis=0)
    kept_rows = jnp.concatenate([blocks[d] for d in order[:half]], axis=0)
    sent = dot32(sent_rows, weight).astype(jnp.bfloat16)
    addends = [dot32(kept_rows, weight).astype(jnp.bfloat16)]
    for bit in bits:
        addends.append(across_ep(sent, 1 << bit))
        rows = addends[-1].shape[0]
        sent = sum(part[rows // 2:rows].astype(jnp.float32) for part in addends).astype(jnp.bfloat16)
    return addends


def dot32(left, right):
    return jnp.dot(left, right, preferred_element_type=jnp.float32)


def call(body, ids, operands, outputs, limit, **more):
    vmem = pl.BlockSpec(memory_space=pltpu.VMEM)
    return pl.pallas_call(
        body,
        in_specs=[pl.BlockSpec(memory_space=pltpu.SMEM)] + [vmem] * len(operands),
        out_specs=[vmem] * len(outputs),
        out_shape=[jax.ShapeDtypeStruct(shape, dtype) for shape, dtype in outputs],
        compiler_params=pltpu.CompilerParams(vmem_limit_bytes=limit << 20),
        **more,
    )(ids, *operands)


def core_column(ids, place, other, quarter):
    return pl.multiple_of((CORES * place + (ids[1] ^ other)) * quarter, 128)


def prepare_body(capacity, ids, routes, routes_t, prob, tokens, rate_param, chosen, combine, scale, decay):
    rows, topk = routes.shape
    slots = chosen.shape[0]
    n_ep = slots // capacity
    down = lax.broadcasted_iota(jnp.int32, (rows, rows), 0)
    across = lax.broadcasted_iota(jnp.int32, (rows, rows), 1)
    earlier = (across < down).astype(jnp.bfloat16)
    earlier_t = (down < across).astype(jnp.bfloat16)
    expert = lax.broadcasted_iota(jnp.int32, (rows, n_ep), 1)
    expert_t = lax.broadcasted_iota(jnp.int32, (n_ep, rows), 0)
    named = [(expert == routes[:, k:k + 1]).astype(jnp.float32) for k in range(topk)]
    named_t = [(expert_t == routes_t[k:k + 1, :]).astype(jnp.float32) for k in range(topk)]
    before = dot32(earlier, sum(named).astype(jnp.bfloat16))
    before_t = dot32(sum(named_t).astype(jnp.bfloat16), earlier_t)
    slot = lax.broadcasted_iota(jnp.int32, (rows, slots), 1)
    slot_t = lax.broadcasted_iota(jnp.int32, (slots, rows), 0)
    total = jnp.sum(prob[...], axis=1, keepdims=True)
    picked, weighted = 0.0, 0.0
    for k in range(topk):
        place = jnp.sum(before * named[k], axis=1, keepdims=True).astype(jnp.int32)
        target = (routes[:, k:k + 1] ^ ids[0]) * capacity + place
        weighted = weighted + jnp.where(slot == target, prob[:, k:k + 1] / total, 0.0)
        place_t = jnp.sum(before_t * named_t[k], axis=0, keepdims=True).astype(jnp.int32)
        target_t = (routes_t[k:k + 1, :] ^ ids[0]) * capacity + place_t
        picked = picked + jnp.where(slot_t == target_t, 1.0, 0.0)
    chosen[...] = picked.astype(jnp.bfloat16)
    high = weighted.astype(jnp.bfloat16)
    combine[:rows, :] = high
    combine[rows:, :] = (weighted - high.astype(jnp.float32)).astype(jnp.bfloat16)
    base = tokens[...].astype(jnp.float32)
    scale[...] = lax.rsqrt(jnp.mean(base * base, axis=-1, keepdims=True) + 1e-06)
    decay[...] = -8.0 * jnp.log1p(jnp.exp(-rate_param[...]))


def unpack_body(half_ep, ids, *refs):
    mine, (theirs, gain, even, odd) = refs[:half_ep], refs[half_ep:]
    rows = mine[0].shape[0]
    own_gain = gain[pl.ds(ids[0], 1), :]
    for core in range(CORES):
        @pl.when(ids[1] == core)
        def _():
            for k in range(half_ep):
                at = slice(k * rows, (k + 1) * rows)
                own, got = (even, odd) if core == 0 else (odd, even)
                own[at, :] = (mine[k][...].astype(jnp.float32) * own_gain).astype(jnp.bfloat16)
                got[at, :] = (theirs[at, :].astype(jnp.float32) * own_gain).astype(jnp.bfloat16)


def mixer_body(n_addends, n_tp, ids, *refs):
    addends_x, addends_y = refs[:n_addends], refs[n_addends:2 * n_addends]
    (
        scale, state_in, history, taps, decay, rate_weight, input_weight, out_weight,
        state_out, window_out, keep, send,
    ) = refs[2 * n_addends:]
    rows = scale.shape[0]
    quarter = out_weight.shape[1] // n_tp
    row_scale = scale[...]
    total = sum(part[:rows, :].astype(jnp.float32) for part in addends_x)
    moved = (total * row_scale).astype(jnp.bfloat16)
    window_out[0] = history[1]
    window_out[1] = history[2]
    window_out[2] = moved
    mixed_in = moved.astype(jnp.float32) * taps[3:4, :].astype(jnp.float32)
    for k in range(3):
        mixed_in = mixed_in + history[k].astype(jnp.float32) * taps[k:k + 1, :].astype(jnp.float32)
    conv = mixed_in.astype(jnp.bfloat16)
    n_blocks, wide = rate_weight.shape[0], rate_weight.shape[1]
    gated = []
    for n in range(n_blocks):
        at = slice(n * wide, (n + 1) * wide)
        part = conv[:, at]
        rate = jax.nn.sigmoid(dot32(part, rate_weight[n]))
        in_gate = jax.nn.sigmoid(dot32(part, input_weight[n]))
        log_decay = rate * decay[:, at]
        twice = 2.0 * log_decay
        series = -twice * (1.0 + twice * (1.0 / 2.0) * (1.0 + twice * (1.0 / 3.0) * (1.0 + twice * (1.0 / 4.0))))
        left = jnp.where(twice > -0.03, series, 1.0 - jnp.exp(twice))
        state = jnp.exp(log_decay) * state_in[:, at] + jnp.sqrt(left) * in_gate * part.astype(jnp.float32)
        state_out[:, at] = state
        proj_y = sum(part[:rows, at].astype(jnp.float32) for part in addends_y) * row_scale
        gated.append((state * jax.nn.gelu(proj_y, approximate=True)).astype(jnp.bfloat16))
    gated = jnp.concatenate(gated, axis=1)
    for other, target in ((1, send), (0, keep)):
        for place in range(n_tp // CORES):
            columns = pl.ds(core_column(ids, place, other, quarter), quarter)
            at = slice(place * quarter, (place + 1) * quarter)
            target[:, at] = dot32(gated, out_weight[:, columns]).astype(jnp.bfloat16)


def merge_body(n_y, ids, tokens, first, second, mixed, squares):
    quarter = first.shape[1] // n_y
    total = 0.0
    for place in range(n_y):
        at = slice(place * quarter, (place + 1) * quarter)
        base = tokens[:, pl.ds(core_column(ids, place, 0, quarter), quarter)].astype(jnp.float32)
        part = base + (first[:, at].astype(jnp.float32) + second[:, at].astype(jnp.float32))
        mixed[:, at] = part
        total = total + jnp.sum(part * part, axis=-1, keepdims=True)
    squares[...] = total


def dispatch_body(n_y, early, ids, mixed, squares, others, gain, chosen, *refs):
    sends, normed = refs[:-1], refs[-1]
    half = mixed.shape[1]
    quarter = half // n_y
    scale = lax.rsqrt((squares[...] + others[...]) / (CORES * half) + 1e-06)
    for place in range(n_y):
        at = slice(place * quarter, (place + 1) * quarter)
        own_gain = gain[:, pl.ds(core_column(ids, place, 0, quarter), quarter)]
        normed[:, at] = (mixed[:, at] * scale * own_gain).astype(jnp.bfloat16)
    capacity = sends[0].shape[0]
    first = early[0] * capacity
    rows = dot32(chosen[:first, :], normed[...]).astype(jnp.bfloat16)
    for d in range(early[0]):
        sends[d][...] = rows[d * capacity:(d + 1) * capacity]
    columns = pl.ds(pl.multiple_of(ids[2] * quarter, 128), quarter)
    rows = dot32(chosen[first:, :], normed[:, columns]).astype(jnp.bfloat16)
    for k, d in enumerate(early):
        sends[d][...] = rows[k * capacity:(k + 1) * capacity]


def expert_body(n_tp, n_pieces, swapped, ids, *refs):
    pieces, (gate, up, down, keep, send) = refs[:CORES * n_pieces], refs[CORES * n_pieces:]
    quarter = gate.shape[1] // n_tp
    n_y = n_tp // CORES
    gate_part, up_part = None, None
    for other in range(CORES):
        for place in range(n_y):
            if n_pieces == 1:
                part = pieces[other][:, place * quarter:(place + 1) * quarter]
            else:
                part = pieces[other * n_pieces + place][...]
            which = (ids[2] ^ place) if swapped else place
            span = pl.ds(core_column(ids, which, other, quarter), quarter)
            term = dot32(part, gate[0, span, :])
            gate_part = term if gate_part is None else gate_part + term
            term = dot32(part, up[0, span, :])
            up_part = term if up_part is None else up_part + term
    hidden = (jax.nn.silu(gate_part) * up_part).astype(jnp.bfloat16)
    for other, target in ((1, send), (0, keep)):
        for place in range(n_y):
            span = pl.ds(core_column(ids, ids[2] ^ place, other, quarter), quarter)
            at = slice(place * quarter, (place + 1) * quarter)
            target[:, at] = dot32(hidden, down[0, :, span]).astype(jnp.bfloat16)


def finish_body(ids, returned, mixed, combine, layer):
    rows, quarter = layer.shape
    base = mixed[:, pl.ds(pl.multiple_of(ids[2] * quarter, 128), quarter)]
    both = dot32(combine[...], returned[...])
    layer[...] = (base + (both[:rows] + both[rows:])).astype(jnp.bfloat16)


def shards(
    tokens,
    state_in,
    conv_in,
    mix_gain,
    rnn_weight,
    gate_weight,
    conv_weight,
    rate_weight,
    input_weight,
    rate_param,
    out_weight,
    moe_gain,
    expert_gate,
    expert_up,
    expert_down,
    routes,
    route_prob,
):
    n_ep, n_tp = lax.axis_size("ep"), lax.axis_size("tp")
    n_y = n_tp // CORES
    e, t = lax.axis_index("ep").astype(jnp.uint32), lax.axis_index("tp").astype(jnp.uint32)
    core, y = t & (CORES - 1), t // CORES
    ids = jnp.stack([e, core, y]).astype(jnp.int32)
    rows, width = tokens.shape
    block, quarter, half = width // n_ep, width // n_tp, width // CORES
    channels = state_in.shape[1]
    n_bits = n_ep.bit_length() - 1
    topk = routes.shape[1]
    capacity = max(2, 2 * rows * topk // n_ep)
    slots = n_ep * capacity
    bf16, f32 = jnp.bfloat16, jnp.float32

    half_ep = n_ep // CORES
    mine = [None] * half_ep
    for k in reversed(range(half_ep)):
        piece = lax.dynamic_slice_in_dim(tokens, (e ^ (CORES * k + core)) * block, block, 1)
        mine[k] = send_to(piece, lambda a, b: (a ^ (CORES * k + b % CORES), b))
    theirs = across_cores(jnp.concatenate(mine, axis=0))
    chosen, combine, scale, decay = call(
        functools.partial(prepare_body, capacity), ids,
        [routes, routes.T, route_prob, tokens, rate_param[None, :]],
        [((slots, rows), bf16), ((2 * rows, slots), bf16), ((rows, 1), f32), ((1, channels), f32)],
        8,
    )
    even, odd = call(
        functools.partial(unpack_body, half_ep), ids,
        [*mine, theirs, mix_gain.reshape(n_ep, block).astype(f32)],
        [((half_ep * rows, block), bf16)] * 2, 8,
    )
    blocks = []
    for k in range(half_ep):
        blocks += [even[k * rows:(k + 1) * rows], odd[k * rows:(k + 1) * rows]]

    bits = list(range(n_bits))
    swapped = [bits[1], bits[0]] + bits[2:]
    addends_x = halving_sum(blocks, rnn_weight, bits)
    addends_y = halving_sum(blocks, gate_weight, swapped)
    state_out, window, keep, send = call(
        functools.partial(mixer_body, len(addends_x), n_tp), ids,
        [
            *addends_x, *addends_y, scale, state_in, jnp.transpose(conv_in, (1, 0, 2)), conv_weight, decay,
            rate_weight, input_weight, out_weight,
        ],
        [((rows, channels), f32), ((3, rows, channels), bf16), ((rows, half), bf16), ((rows, half), bf16)],
        20,
    )
    conv_out = jnp.transpose(window, (1, 0, 2))

    first = (keep.astype(f32) + across_cores(send).astype(f32)).astype(bf16)
    second = across_y(first, 1)
    offset = 2
    while offset < n_y:
        first = (first.astype(f32) + second.astype(f32)).astype(bf16)
        second = across_y(first, offset)
        offset *= 2
    mixed, squares = call(
        functools.partial(merge_body, n_y), ids, [tokens, first, second],
        [((rows, half), f32), ((rows, 1), f32)], 8,
    )
    near = list(range(n_ep // 2))
    early = list(range(3 * n_ep // 4, n_ep))
    late = list(range(n_ep // 2, 3 * n_ep // 4))
    sends = pl.pallas_call(
        functools.partial(dispatch_body, n_y, early),
        in_specs=[pl.BlockSpec(memory_space=pltpu.SMEM)] + [pl.BlockSpec(memory_space=pltpu.VMEM)] * 5,
        out_specs=[pl.BlockSpec(memory_space=pltpu.VMEM)] * n_ep,
        out_shape=[
            jax.ShapeDtypeStruct((capacity, quarter if d in early else half), bf16) for d in range(n_ep)
        ],
        scratch_shapes=[pltpu.VMEM((rows, half), bf16)],
        compiler_params=pltpu.CompilerParams(vmem_limit_bytes=8 << 20),
        name="dispatch",
    )(ids, mixed, squares, across_cores(squares), moe_gain[None, :].astype(f32), chosen)

    landed = {0: sends[0]}
    for group in (early, near[1:], late):
        for d in reversed(group):
            landed[d] = across_ep(sends[d], d)
    back = {}
    for name, group in (("near", near), ("early", early), ("late", late)):
        pieces = [jnp.concatenate([landed[d] for d in group], axis=0)]
        if name == "early":
            pieces += [across_y(pieces[0], k) for k in range(1, n_y)]
        others = [across_cores(piece) for piece in pieces]
        count = len(group) * capacity
        keep, send = call(
            functools.partial(expert_body, n_tp, len(pieces), name == "early"), ids,
            [*pieces, *others, expert_gate, expert_up, expert_down], [((count, half), bf16)] * 2,
            20,
            cost_estimate=pl.CostEstimate(
                flops=6 * count * width * expert_gate.shape[2], bytes_accessed=0, transcendentals=0
            ),
        )
        summed = (keep.astype(f32) + across_cores(send).astype(f32)).astype(bf16)
        total = summed[:, :quarter].astype(f32)
        for k in range(1, n_y):
            total = total + across_y(summed[:, k * quarter:(k + 1) * quarter], k).astype(f32)
        total = total.astype(bf16)
        for place in reversed(range(len(group))):
            d = group[place]
            piece = total[place * capacity:(place + 1) * capacity]
            back[d] = across_ep(piece, d) if d else piece
    (layer_out,) = call(
        finish_body, ids, [jnp.concatenate([back[d] for d in range(n_ep)], axis=0), mixed, combine],
        [((rows, quarter), bf16)], 8,
    )
    return (layer_out, state_out, conv_out)


def solution(mesh):
    in_specs = (
        P("ep", None),
        P("ep", "tp"),
        P("ep", None, "tp"),
        P(),
        P("ep", "tp"),
        P("ep", "tp"),
        P(None, "tp"),
        P("tp", None, None),
        P("tp", None, None),
        P("tp"),
        P("tp", None),
        P(),
        P("ep", None, "tp"),
        P("ep", None, "tp"),
        P("ep", "tp", None),
        P("ep", None),
        P("ep", None),
    )
    out_specs = (P("ep", "tp"), P("ep", "tp"), P("ep", None, "tp"))
    return jax.shard_map(shards, mesh=mesh, in_specs=in_specs, out_specs=out_specs, check_vma=False)
```

time: 269 us -> 144 us (0.54)
  waiting for transfers between devices: 142 us -> 60.8 us
  blocking collectives: 74.4 us -> 0 us
  starting transfers between devices: 5.64 us -> 43.7 us
  Pallas kernels: 0 us -> 16.9 us
  matrix products: 16.6 us -> 1.78 us
  between operations: 14.1 us -> 1.11 us
  local copies, waits for them, and re-layouts: 3.75 us -> 16.4 us
  other arithmetic: 11.2 us -> 2.13 us
    reduce_scatter x2 -> x0, waiting for transfers between devices: 96.6 us -> none  [the longest x1 66.8 us: shards(): lax.psum_scatter(jnp.dot(columns, joined, preferred_element_type=jnp.floa...]
    all_to_all x2 -> x0, blocking collectives: 74.4 us -> none  [the longest x1 52.8 us: shards(): lax.all_to_all(send, 'ep', split_axis=0, concat_axis=0, tiled=True)]
    ppermute x0 -> x39, waiting for transfers between devices: none -> 60.8 us  [send_to(): return lax.ppermute(value, AXES, pairs)]
    ppermute x0 -> x39, starting transfers between devices: none -> 43.7 us  [send_to(): return lax.ppermute(value, AXES, pairs)]
    psum x1 -> x0, waiting for transfers between devices: 32.4 us -> none  [shards(): lax.psum(partial_out.astype(jnp.bfloat16), 'tp').astype(jnp.float32)]
    pallas_call x0 -> x9, Pallas kernels: none -> 16.9 us  [the longest x8 15.9 us: call(): pl.pallas_call(body, in_specs=[pl.BlockSpec(memory_space=pltpu.SMEM)] + [...]
    dot_general x9 -> x4, matrix products: 16.6 us -> 1.78 us  [dot32(): return jnp.dot(left, right, preferred_element_type=jnp.float32)]
    all_to_all x1 -> x0, waiting for transfers between devices: 13.3 us -> none  [shards(): lax.all_to_all(reduced, 'ep', split_axis=0, concat_axis=0, tiled=True)]
  transfers between devices with their start and end apart: 4 -> 39, of which waited for: 4 -> 20; matrix products, arithmetic and copies ran while one was open for 1% -> 5% of each run, Pallas kernels for 0% -> 6%
where the time goes in v1:
time: 144 us; the launch traced here: 143 us
  waiting for transfers between devices  60.8 us (42%)
  starting transfers between devices  43.7 us (30%)
  Pallas kernels  16.9 us (12%)
  local copies, waits for them, and re-layouts  16.4 us (11%)
  other arithmetic  2.13 us (1%)
  matrix products  1.78 us (1%)
    ppermute x39, waiting for transfers between devices, send_to(): return lax.ppermute(value, AXES, pairs)  60.8 us
    ppermute x39, starting transfers between devices, send_to(): return lax.ppermute(value, AXES, pairs)  43.7 us
    pallas_call x8, Pallas kernels, call(): pl.pallas_call(body, in_specs=[pl.BlockSpec(memory_space=pltpu.SMEM)] + [...  15.9 us
    unnamed x57, local copies, waits for them, and re-layouts  14.5 us
  transfers between devices with their start and end apart: 39, of which 20 were waited for; matrix products, arithmetic and copies ran while one was open for 5% of the time, Pallas kernels for 6%

profile of v1, /device:TPU:0, one launch (start us, length us, event | category | flops | bytes accessed | tf_op | source)
XLA Modules:
  0.0 142.9 jit_solution(17746802399262490898)
XLA Ops:
  2.4 3.1 %collective-permute-start.1 = (bf16[64,512]{1,0:T(8,128)(2,1)S(1)}, bf16[64,512]{1,0:T(8,128)(2,1)S(1)}, u32[]{:S(2)}, u32[]{:S(2)}) collective-permute-start(bf16[64,512]{1,0:T(8,128)(2,1)S(1)} %get-tuple-element.57), channel_id=1, source_target_pairs={{0,8},{1,13},{2,10},{3,15},{4,12},{5,9},{6,14},{7,11},{8,0},{9,5},... | collective-permute-start | bytes 196616 | tf_op jit(solution)/shard_map/ppermute | solution.py:22
  5.6 2.6 %collective-permute-start.2 = (bf16[64,512]{1,0:T(8,128)(2,1)S(1)}, bf16[64,512]{1,0:T(8,128)(2,1)S(1)}, u32[]{:S(2)}, u32[]{:S(2)}) collective-permute-start(bf16[64,512]{1,0:T(8,128)(2,1)S(1)} %get-tuple-element.56), channel_id=1, source_target_pairs={{0,16},{1,21},{2,18},{3,23},{4,20},{5,17},{6,22},{7,19},{8,24},{9,... | collective-permute-start | bytes 196616 | tf_op jit(solution)/shard_map/ppermute | solution.py:22
  8.2 3.3 %collective-permute-done.2.refs_2_ = bf16[64,512]{1,0:T(8,128)(2,1)S(1)} collective-permute-done((bf16[64,512]{1,0:T(8,128)(2,1)S(1)}, bf16[64,512]{1,0:T(8,128)(2,1)S(1)}, u32[]{:S(2)}, u32[]{:S(2)}) %collective-permute-start.2) | collective-permute-done | bytes 65568 | tf_op jit(solution)/shard_map/ppermute | solution.py:22
  11.4 2.9 %collective-permute-done.3.refs_3_ = bf16[64,512]{1,0:T(8,128)(2,1)S(1)} collective-permute-done((bf16[64,512]{1,0:T(8,128)(2,1)S(1)}, bf16[64,512]{1,0:T(8,128)(2,1)S(1)}, u32[]{:S(2)}, u32[]{:S(2)}) %collective-permute-start.3) | collective-permute-done | bytes 65568 | tf_op jit(solution)/shard_map/ppermute | solution.py:22
  14.3 2.3 %collective-permute-start.4 = (bf16[256,512]{1,0:T(8,128)(2,1)S(1)}, bf16[256,512]{1,0:T(8,128)(2,1)S(1)}, u32[]{:S(2)}, u32[]{:S(2)}) collective-permute-start(bf16[256,512]{1,0:T(8,128)(2,1)S(1)} %pad_maximum_fusion.6), channel_id=1, source_target_pairs={{0,1},{1,0},{2,3},{3,2},{4,5},{5,4},{6,7},{7,6},{8,9},{9,8},{10,11... | collective-permute-start | bytes 786440 | tf_op jit(solution)/shard_map/ppermute | solution.py:22
  21.1 12.2 %collective-permute-done.8.refs_5_ = bf16[256,1024]{1,0:T(8,128)(2,1)S(1)} collective-permute-done((bf16[256,1024]{1,0:T(8,128)(2,1)S(1)}, bf16[256,1024]{1,0:T(8,128)(2,1)S(1)}, u32[]{:S(2)}, u32[]{:S(2)}) %collective-permute-start.8) | collective-permute-done | bytes 524320 | tf_op jit(solution)/shard_map/ppermute | solution.py:22
  35.7 5.4 %collective-permute-done.9.refs_6_ = bf16[128,1024]{1,0:T(8,128)(2,1)S(1)} collective-permute-done((bf16[128,1024]{1,0:T(8,128)(2,1)S(1)}, bf16[128,1024]{1,0:T(8,128)(2,1)S(1)}, u32[]{:S(2)}, u32[]{:S(2)}) %collective-permute-start.9) | collective-permute-done | bytes 262176 | tf_op jit(solution)/shard_map/ppermute | solution.py:22
  53.3 2.3 %collective-permute-done.7.refs_3_ = bf16[64,1024]{1,0:T(8,128)(2,1)} collective-permute-done((bf16[64,1024]{1,0:T(8,128)(2,1)}, bf16[64,1024]{1,0:T(8,128)(2,1)}, u32[]{:S(2)}, u32[]{:S(2)}) %collective-permute-start.7) | collective-permute-done | bytes 131104 | tf_op jit(solution)/shard_map/ppermute | solution.py:22
  55.6 3.4 %copy-done.4 = bf16[1024,4096]{1,0:T(8,128)(2,1)S(1)} copy-done((bf16[1024,4096]{1,0:T(8,128)(2,1)S(1)}, bf16[1024,4096]{1,0:T(8,128)(2,1)}, u32[]{:S(2)}) %copy-start.4) | copy-done | bytes 8388632
  65.0 3.9 %shard_map.186 = (f32[64,1024]{1,0:T(8,128)}, bf16[3,64,1024]{2,1,0:T(8,128)(2,1)}, bf16[64,2048]{1,0:T(8,128)(2,1)S(1)}, bf16[64,2048]{1,0:T(8,128)(2,1)S(1)}) custom-call(s32[3]{0:T(128)S(1)} %add_convert_fusion.11.ids, bf16[256,1024]{1,0:T(8,128)(2,1)S(1)} %copy-done.7, bf16[256,1024]{1,0:T(8,128)(2,1)S(1)} %collective-permute-done.5.refs_1_, ...), custom_call_target="tpu_custom_call" | custom-call | tf_op jit(solution)/shard_map/pallas_call | solution.py:59
  72.1 6.8 %collective-permute-done.12.second = bf16[64,2048]{1,0:T(8,128)(2,1)S(1)} collective-permute-done((bf16[64,2048]{1,0:T(8,128)(2,1)S(1)}, bf16[64,2048]{1,0:T(8,128)(2,1)S(1)}, u32[]{:S(2)}, u32[]{:S(2)}) %collective-permute-start.12) | collective-permute-done | bytes 262176 | tf_op jit(solution)/shard_map/ppermute | solution.py:22
  83.6 2.2 %collective-permute-start.31 = (bf16[32,1024]{1,0:T(8,128)(2,1)S(1)}, bf16[32,1024]{1,0:T(8,128)(2,1)S(1)}, u32[]{:S(2)}, u32[]{:S(2)}) collective-permute-start(bf16[32,1024]{1,0:T(8,128)(2,1)S(1)} %get-tuple-element.49), channel_id=1, source_target_pairs={{0,28},{1,29},{2,30},{3,31},{4,24},{5,25},{6,26},{7,27},{8,20},{9,... | collective-permute-start | bytes 196616 | tf_op jit(solution)/shard_map/ppermute | solution.py:22
  85.8 3.8 %collective-permute-start.24 = (bf16[32,2048]{1,0:T(8,128)(2,1)S(1)}, bf16[32,2048]{1,0:T(8,128)(2,1)S(1)}, u32[]{:S(2)}, u32[]{:S(2)}) collective-permute-start(bf16[32,2048]{1,0:T(8,128)(2,1)S(1)} %get-tuple-element.45), channel_id=1, source_target_pairs={{0,20},{1,21},{2,22},{3,23},{4,16},{5,17},{6,18},{7,19},{8,28},{9,... | collective-permute-start | bytes 393224 | tf_op jit(solution)/shard_map/ppermute | solution.py:22
  93.3 4.7 %collective-permute-done.23 = bf16[32,2048]{1,0:T(8,128)(2,1)S(1)} collective-permute-done((bf16[32,2048]{1,0:T(8,128)(2,1)S(1)}, bf16[32,2048]{1,0:T(8,128)(2,1)S(1)}, u32[]{:S(2)}, u32[]{:S(2)}) %collective-permute-start.23) | collective-permute-done | bytes 131104 | tf_op jit(solution)/shard_map/ppermute | solution.py:22
  99.5 2.0 %collective-permute-done.24 = bf16[32,2048]{1,0:T(8,128)(2,1)S(1)} collective-permute-done((bf16[32,2048]{1,0:T(8,128)(2,1)S(1)}, bf16[32,2048]{1,0:T(8,128)(2,1)S(1)}, u32[]{:S(2)}, u32[]{:S(2)}) %collective-permute-start.24) | collective-permute-done | bytes 131104 | tf_op jit(solution)/shard_map/ppermute | solution.py:22
  104.7 2.9 %shard_map.190 = (bf16[64,2048]{1,0:T(8,128)(2,1)S(1)}, bf16[64,2048]{1,0:T(8,128)(2,1)S(1)}) custom-call(s32[3]{0:T(128)S(1)} %add_convert_fusion.11.ids, bf16[64,1024]{1,0:T(8,128)(2,1)S(1)} %constant_dynamic-update-slice_fusion.6.refs_0_, bf16[64,1024]{1,0:T(8,128)(2,1)S(1)} %collective-permute-done.32.refs_1_, ...), custom_call_target="tpu_custom_call" | custom-call | flops 805306368 | tf_op jit(solution)/shard_map/pallas_call | solution.py:59
  108.2 2.9 %shard_map.189 = (bf16[64,2048]{1,0:T(8,128)(2,1)S(1)}, bf16[64,2048]{1,0:T(8,128)(2,1)S(1)}) custom-call(s32[3]{0:T(128)S(1)} %add_convert_fusion.11.ids, bf16[64,2048]{1,0:T(8,128)(2,1)S(1)} %constant_dynamic-update-slice_fusion.4.refs_0_, bf16[64,2048]{1,0:T(8,128)(2,1)S(1)} %collective-permute-done.25.refs_1_, bf16[1,4096,512]{2,1,0:T(8,128)(2,1)S(1)} %copy-done.1, ...), custom_call_target="tpu_custom_call" | custom-call | flops 805306368 | tf_op jit(solution)/shard_map/pallas_call | solution.py:59
  113.0 2.5 %shard_map.188 = (bf16[128,2048]{1,0:T(8,128)(2,1)S(1)}, bf16[128,2048]{1,0:T(8,128)(2,1)S(1)}) custom-call(s32[3]{0:T(128)S(1)} %add_convert_fusion.11.ids, bf16[128,2048]{1,0:T(8,128)(2,1)S(1)} %constant_dynamic-update-slice_fusion.refs_0_, bf16[128,2048]{1,0:T(8,128)(2,1)S(1)} %collective-permute-done.17.refs_1_, bf16[1,4096,512]{2,1,0:T(8,128)(2,1)S(1)} %copy-done.1, ...), custom_call_target="tpu_custom_call" | custom-call | flops 1610612736 | tf_op jit(solution)/shard_map/pallas_call | solution.py:59
  119.1 2.1 %collective-permute-start.37 = (bf16[32,1024]{1,0:T(8,128)(2,1)S(1)}, bf16[32,1024]{1,0:T(8,128)(2,1)S(1)}, u32[]{:S(2)}, u32[]{:S(2)}) collective-permute-start(bf16[32,1024]{1,0:T(8,128)(2,1)S(1)} %get-tuple-element.72), channel_id=1, source_target_pairs={{0,24},{1,25},{2,26},{3,27},{4,28},{5,29},{6,30},{7,31},{8,16},{9,... | collective-permute-start | bytes 196616 | tf_op jit(solution)/shard_map/ppermute | solution.py:22
  121.2 2.6 %collective-permute-start.38 = (bf16[32,1024]{1,0:T(8,128)(2,1)S(1)}, bf16[32,1024]{1,0:T(8,128)(2,1)S(1)}, u32[]{:S(2)}, u32[]{:S(2)}) collective-permute-start(bf16[32,1024]{1,0:T(8,128)(2,1)S(1)} %get-tuple-element.71), channel_id=1, source_target_pairs={{0,28},{1,29},{2,30},{3,31},{4,24},{5,25},{6,26},{7,27},{8,20},{9,... | collective-permute-start | bytes 196616 | tf_op jit(solution)/shard_map/ppermute | solution.py:22
  123.8 3.5 %collective-permute-done.19 = bf16[128,1024]{1,0:T(8,128)(2,1)S(1)} collective-permute-done((bf16[128,1024]{1,0:T(8,128)(2,1)S(1)}, bf16[128,1024]{1,0:T(8,128)(2,1)S(1)}, u32[]{:S(2)}, u32[]{:S(2)}) %collective-permute-start.19) | collective-permute-done | bytes 262176 | tf_op jit(solution)/shard_map/ppermute | solution.py:22
  128.8 3.1 %collective-permute-start.29 = (bf16[32,1024]{1,0:T(8,128)(2,1)S(1)}, bf16[32,1024]{1,0:T(8,128)(2,1)S(1)}, u32[]{:S(2)}, u32[]{:S(2)}) collective-permute-start(bf16[32,1024]{1,0:T(8,128)(2,1)S(1)} %get-tuple-element.73), channel_id=1, source_target_pairs={{0,20},{1,21},{2,22},{3,23},{4,16},{5,17},{6,18},{7,19},{8,28},{9,... | collective-permute-start | bytes 196616 | tf_op jit(solution)/shard_map/ppermute | solution.py:22
  131.9 4.4 %collective-permute-done.21 = bf16[32,1024]{1,0:T(8,128)(2,1)S(1)} collective-permute-done((bf16[32,1024]{1,0:T(8,128)(2,1)S(1)}, bf16[32,1024]{1,0:T(8,128)(2,1)S(1)}, u32[]{:S(2)}, u32[]{:S(2)}) %collective-permute-start.21) | collective-permute-done | bytes 65568 | tf_op jit(solution)/shard_map/ppermute | solution.py:22
  137.6 3.8 %collective-permute-done.22 = bf16[32,1024]{1,0:T(8,128)(2,1)S(1)} collective-permute-done((bf16[32,1024]{1,0:T(8,128)(2,1)S(1)}, bf16[32,1024]{1,0:T(8,128)(2,1)S(1)}, u32[]{:S(2)}, u32[]{:S(2)}) %collective-permute-start.22) | collective-permute-done | bytes 65568 | tf_op jit(solution)/shard_map/ppermute | solution.py:22
  (151 shorter events, 53.3 us)
Async XLA Ops:
  1.8 6.4 %collective-permute-start = (bf16[64,512]{1,0:T(8,128)(2,1)S(1)}, bf16[64,512]{1,0:T(8,128)(2,1)S(1)}, u32[]{:S(2)}, u32[]{:S(2)}) collective-permute-start(bf16[64,512]{1,0:T(8,128)(2,1)S(1)} %get-tuple-element.58), channel_id=1, source_target_pairs={{0,0},{1,5},{2,2},{3,7},{4,4},{5,1},{6,6},{7,3},{8,8},{9,13},{10,1... | collective-permute-start | bytes 196616 | tf_op jit(solution)/shard_map/ppermute | solution.py:22
  5.6 5.9 %collective-permute-start.2 = (bf16[64,512]{1,0:T(8,128)(2,1)S(1)}, bf16[64,512]{1,0:T(8,128)(2,1)S(1)}, u32[]{:S(2)}, u32[]{:S(2)}) collective-permute-start(bf16[64,512]{1,0:T(8,128)(2,1)S(1)} %get-tuple-element.56), channel_id=1, source_target_pairs={{0,16},{1,21},{2,18},{3,23},{4,20},{5,17},{6,22},{7,19},{8,24},{9,... | collective-permute-start | bytes 196616 | tf_op jit(solution)/shard_map/ppermute | solution.py:22
  8.2 6.2 %collective-permute-start.3 = (bf16[64,512]{1,0:T(8,128)(2,1)S(1)}, bf16[64,512]{1,0:T(8,128)(2,1)S(1)}, u32[]{:S(2)}, u32[]{:S(2)}) collective-permute-start(bf16[64,512]{1,0:T(8,128)(2,1)S(1)} %get-tuple-element.55), channel_id=1, source_target_pairs={{0,24},{1,29},{2,26},{3,31},{4,28},{5,25},{6,30},{7,27},{8,16},{9,... | collective-permute-start | bytes 196616 | tf_op jit(solution)/shard_map/ppermute | solution.py:22
  19.0 14.3 %collective-permute-start.8 = (bf16[256,1024]{1,0:T(8,128)(2,1)S(1)}, bf16[256,1024]{1,0:T(8,128)(2,1)S(1)}, u32[]{:S(2)}, u32[]{:S(2)}) collective-permute-start(bf16[256,1024]{1,0:T(8,128)(2,1)S(1)} %convolution_convert_fusion), channel_id=1, source_target_pairs={{0,8},{1,9},{2,10},{3,11},{4,12},{5,13},{6,14},{7,15},{8,0},{9,1},... | collective-permute-start | bytes 1572872 | tf_op jit(solution)/shard_map/ppermute | solution.py:22
  19.6 14.4 %collective-permute-start.5 = (bf16[256,1024]{1,0:T(8,128)(2,1)S(1)}, bf16[256,1024]{1,0:T(8,128)(2,1)S(1)}, u32[]{:S(2)}, u32[]{:S(2)}) collective-permute-start(bf16[256,1024]{1,0:T(8,128)(2,1)S(1)} %convolution_convert_fusion.2), channel_id=1, source_target_pairs={{0,4},{1,5},{2,6},{3,7},{4,0},{5,1},{6,2},{7,3},{8,12},{9,13},{10,... | collective-permute-start | bytes 1572872 | tf_op jit(solution)/shard_map/ppermute | solution.py:22
  33.3 7.8 %collective-permute-start.9 = (bf16[128,1024]{1,0:T(8,128)(2,1)S(1)}, bf16[128,1024]{1,0:T(8,128)(2,1)S(1)}, u32[]{:S(2)}, u32[]{:S(2)}) collective-permute-start(bf16[128,1024]{1,0:T(8,128)(2,1)S(1)} %add_convert_fusion.5), channel_id=1, source_target_pairs={{0,4},{1,5},{2,6},{3,7},{4,0},{5,1},{6,2},{7,3},{8,12},{9,13},{10,... | collective-permute-start | bytes 786440 | tf_op jit(solution)/shard_map/ppermute | solution.py:22
  34.0 9.2 %collective-permute-start.6 = (bf16[128,1024]{1,0:T(8,128)(2,1)S(1)}, bf16[128,1024]{1,0:T(8,128)(2,1)S(1)}, u32[]{:S(2)}, u32[]{:S(2)}) collective-permute-start(bf16[128,1024]{1,0:T(8,128)(2,1)S(1)} %add_convert_fusion.6), channel_id=1, source_target_pairs={{0,8},{1,9},{2,10},{3,11},{4,12},{5,13},{6,14},{7,15},{8,0},{9,1},... | collective-permute-start | bytes 786440 | tf_op jit(solution)/shard_map/ppermute | solution.py:22
  41.8 11.4 %collective-permute-start.10 = (bf16[64,1024]{1,0:T(8,128)(2,1)}, bf16[64,1024]{1,0:T(8,128)(2,1)S(1)}, u32[]{:S(2)}, u32[]{:S(2)}) collective-permute-start(bf16[64,1024]{1,0:T(8,128)(2,1)} %add_convert_fusion.9), channel_id=1, source_target_pairs={{0,16},{1,17},{2,18},{3,19},{4,20},{5,21},{6,22},{7,23},{8,24},{9,... | collective-permute-start | bytes 393224 | tf_op jit(solution)/shard_map/ppermute | solution.py:22
  44.0 11.6 %collective-permute-start.7 = (bf16[64,1024]{1,0:T(8,128)(2,1)}, bf16[64,1024]{1,0:T(8,128)(2,1)}, u32[]{:S(2)}, u32[]{:S(2)}) collective-permute-start(bf16[64,1024]{1,0:T(8,128)(2,1)} %add_convert_fusion.10), channel_id=1, source_target_pairs={{0,16},{1,17},{2,18},{3,19},{4,20},{5,21},{6,22},{7,23},{8,24},{9,... | collective-permute-start | bytes 393224 | tf_op jit(solution)/shard_map/ppermute | solution.py:22
  70.5 8.4 %collective-permute-start.12 = (bf16[64,2048]{1,0:T(8,128)(2,1)S(1)}, bf16[64,2048]{1,0:T(8,128)(2,1)S(1)}, u32[]{:S(2)}, u32[]{:S(2)}) collective-permute-start(bf16[64,2048]{1,0:T(8,128)(2,1)S(1)} %add_convert_fusion.4.first), channel_id=1, source_target_pairs={{0,2},{1,3},{2,0},{3,1},{4,6},{5,7},{6,4},{7,5},{8,10},{9,11},{10,... | collective-permute-start | bytes 786440 | tf_op jit(solution)/shard_map/ppermute | solution.py:22
  81.9 8.3 %collective-permute-start.30 = (bf16[32,1024]{1,0:T(8,128)(2,1)S(1)}, bf16[32,1024]{1,0:T(8,128)(2,1)S(1)}, u32[]{:S(2)}, u32[]{:S(2)}) collective-permute-start(bf16[32,1024]{1,0:T(8,128)(2,1)S(1)} %get-tuple-element.48), channel_id=1, source_target_pairs={{0,24},{1,25},{2,26},{3,27},{4,28},{5,29},{6,30},{7,31},{8,16},{9,... | collective-permute-start | bytes 196616 | tf_op jit(solution)/shard_map/ppermute | solution.py:22
  83.6 7.8 %collective-permute-start.31 = (bf16[32,1024]{1,0:T(8,128)(2,1)S(1)}, bf16[32,1024]{1,0:T(8,128)(2,1)S(1)}, u32[]{:S(2)}, u32[]{:S(2)}) collective-permute-start(bf16[32,1024]{1,0:T(8,128)(2,1)S(1)} %get-tuple-element.49), channel_id=1, source_target_pairs={{0,28},{1,29},{2,30},{3,31},{4,24},{5,25},{6,26},{7,27},{8,20},{9,... | collective-permute-start | bytes 196616 | tf_op jit(solution)/shard_map/ppermute | solution.py:22
  85.8 12.2 %collective-permute-start.23 = (bf16[32,2048]{1,0:T(8,128)(2,1)S(1)}, bf16[32,2048]{1,0:T(8,128)(2,1)S(1)}, u32[]{:S(2)}, u32[]{:S(2)}) collective-permute-start(bf16[32,2048]{1,0:T(8,128)(2,1)S(1)} %get-tuple-element.44), channel_id=1, source_target_pairs={{0,16},{1,17},{2,18},{3,19},{4,20},{5,21},{6,22},{7,23},{8,24},{9,... | collective-permute-start | bytes 393224 | tf_op jit(solution)/shard_map/ppermute | solution.py:22
  85.8 15.7 %collective-permute-start.24 = (bf16[32,2048]{1,0:T(8,128)(2,1)S(1)}, bf16[32,2048]{1,0:T(8,128)(2,1)S(1)}, u32[]{:S(2)}, u32[]{:S(2)}) collective-permute-start(bf16[32,2048]{1,0:T(8,128)(2,1)S(1)} %get-tuple-element.45), channel_id=1, source_target_pairs={{0,20},{1,21},{2,22},{3,23},{4,16},{5,17},{6,18},{7,19},{8,28},{9,... | collective-permute-start | bytes 393224 | tf_op jit(solution)/shard_map/ppermute | solution.py:22
  89.6 11.9 %collective-permute-start.14 = (bf16[32,2048]{1,0:T(8,128)(2,1)S(1)}, bf16[32,2048]{1,0:T(8,128)(2,1)S(1)}, u32[]{:S(2)}, u32[]{:S(2)}) collective-permute-start(bf16[32,2048]{1,0:T(8,128)(2,1)S(1)} %get-tuple-element.39), channel_id=1, source_target_pairs={{0,4},{1,5},{2,6},{3,7},{4,0},{5,1},{6,2},{7,3},{8,12},{9,13},{10,... | collective-permute-start | bytes 393224 | tf_op jit(solution)/shard_map/ppermute | solution.py:22
  90.3 13.0 %collective-permute-start.15 = (bf16[32,2048]{1,0:T(8,128)(2,1)S(1)}, bf16[32,2048]{1,0:T(8,128)(2,1)S(1)}, u32[]{:S(2)}, u32[]{:S(2)}) collective-permute-start(bf16[32,2048]{1,0:T(8,128)(2,1)S(1)} %get-tuple-element.40), channel_id=1, source_target_pairs={{0,8},{1,9},{2,10},{3,11},{4,12},{5,13},{6,14},{7,15},{8,0},{9,1},... | collective-permute-start | bytes 393224 | tf_op jit(solution)/shard_map/ppermute | solution.py:22
  91.3 16.5 %collective-permute-start.16 = (bf16[32,2048]{1,0:T(8,128)(2,1)S(1)}, bf16[32,2048]{1,0:T(8,128)(2,1)S(1)}, u32[]{:S(2)}, u32[]{:S(2)}) collective-permute-start(bf16[32,2048]{1,0:T(8,128)(2,1)S(1)} %get-tuple-element.41), channel_id=1, source_target_pairs={{0,12},{1,13},{2,14},{3,15},{4,8},{5,9},{6,10},{7,11},{8,4},{9,5},... | collective-permute-start | bytes 393224 | tf_op jit(solution)/shard_map/ppermute | solution.py:22
  101.5 6.7 %collective-permute-start.25 = (bf16[64,2048]{1,0:T(8,128)(2,1)S(1)}, bf16[64,2048]{1,0:T(8,128)(2,1)S(1)}, u32[]{:S(2)}, u32[]{:S(2)}) collective-permute-start(bf16[64,2048]{1,0:T(8,128)(2,1)S(1)} %constant_dynamic-update-slice_fusion.4.refs_0_), channel_id=1, source_target_pairs={{0,1},{1,0},{2,3},{3,2},{4,5},{5,4},{6,7},{7,6},{8,9},{9,8},{10,11... | collective-permute-start | bytes 786440 | tf_op jit(solution)/shard_map/ppermute | solution.py:22
  115.7 8.0 %collective-permute-start.27 = (bf16[64,1024]{1,0:T(8,128)(2,1)S(1)}, bf16[64,1024]{1,0:T(8,128)(2,1)S(1)}, u32[]{:S(2)}, u32[]{:S(2)}) collective-permute-start(bf16[64,1024]{1,0:T(8,128)(2,1)S(1)} %slice.145), channel_id=1, source_target_pairs={{0,2},{1,3},{2,0},{3,1},{4,6},{5,7},{6,4},{7,5},{8,10},{9,11},{10,... | collective-permute-start | bytes 393224 | tf_op jit(solution)/shard_map/ppermute | solution.py:22
  117.6 9.6 %collective-permute-start.19 = (bf16[128,1024]{1,0:T(8,128)(2,1)S(1)}, bf16[128,1024]{1,0:T(8,128)(2,1)S(1)}, u32[]{:S(2)}, u32[]{:S(2)}) collective-permute-start(bf16[128,1024]{1,0:T(8,128)(2,1)S(1)} %slice.139), channel_id=1, source_target_pairs={{0,2},{1,3},{2,0},{3,1},{4,6},{5,7},{6,4},{7,5},{8,10},{9,11},{10,... | collective-permute-start | bytes 786440 | tf_op jit(solution)/shard_map/ppermute | solution.py:22
  119.1 22.4 %collective-permute-start.37 = (bf16[32,1024]{1,0:T(8,128)(2,1)S(1)}, bf16[32,1024]{1,0:T(8,128)(2,1)S(1)}, u32[]{:S(2)}, u32[]{:S(2)}) collective-permute-start(bf16[32,1024]{1,0:T(8,128)(2,1)S(1)} %get-tuple-element.72), channel_id=1, source_target_pairs={{0,24},{1,25},{2,26},{3,27},{4,28},{5,29},{6,30},{7,31},{8,16},{9,... | collective-permute-start | bytes 196616 | tf_op jit(solution)/shard_map/ppermute | solution.py:22
  121.2 20.3 %collective-permute-start.38 = (bf16[32,1024]{1,0:T(8,128)(2,1)S(1)}, bf16[32,1024]{1,0:T(8,128)(2,1)S(1)}, u32[]{:S(2)}, u32[]{:S(2)}) collective-permute-start(bf16[32,1024]{1,0:T(8,128)(2,1)S(1)} %get-tuple-element.71), channel_id=1, source_target_pairs={{0,28},{1,29},{2,30},{3,31},{4,24},{5,25},{6,26},{7,27},{8,20},{9,... | collective-permute-start | bytes 196616 | tf_op jit(solution)/shard_map/ppermute | solution.py:22
  128.7 12.7 %collective-permute-start.28 = (bf16[32,1024]{1,0:T(8,128)(2,1)S(1)}, bf16[32,1024]{1,0:T(8,128)(2,1)S(1)}, u32[]{:S(2)}, u32[]{:S(2)}) collective-permute-start(bf16[32,1024]{1,0:T(8,128)(2,1)S(1)} %get-tuple-element.74), channel_id=1, source_target_pairs={{0,16},{1,17},{2,18},{3,19},{4,20},{5,21},{6,22},{7,23},{8,24},{9,... | collective-permute-start | bytes 196616 | tf_op jit(solution)/shard_map/ppermute | solution.py:22
  128.8 12.6 %collective-permute-start.29 = (bf16[32,1024]{1,0:T(8,128)(2,1)S(1)}, bf16[32,1024]{1,0:T(8,128)(2,1)S(1)}, u32[]{:S(2)}, u32[]{:S(2)}) collective-permute-start(bf16[32,1024]{1,0:T(8,128)(2,1)S(1)} %get-tuple-element.73), channel_id=1, source_target_pairs={{0,20},{1,21},{2,22},{3,23},{4,16},{5,17},{6,18},{7,19},{8,28},{9,... | collective-permute-start | bytes 196616 | tf_op jit(solution)/shard_map/ppermute | solution.py:22
  (37 other events, 357.1 us)

commit v2 on v1

--- a/solution.py
+++ b/solution.py
@@ -10,6 +10,7 @@
 
 AXES = ("ep", "tp")
 CORES = 2
+CHUNKS = 2
 
 
 def send_to(value, target):
@@ -41,13 +42,18 @@
     half = len(order) // 2
     sent_rows = jnp.concatenate([blocks[d] for d in order[half:]], axis=0)
     kept_rows = jnp.concatenate([blocks[d] for d in order[:half]], axis=0)
-    sent = dot32(sent_rows, weight).astype(jnp.bfloat16)
-    addends = [dot32(kept_rows, weight).astype(jnp.bfloat16)]
-    for bit in bits:
-        addends.append(across_ep(sent, 1 << bit))
-        rows = addends[-1].shape[0]
-        sent = sum(part[rows // 2:rows].astype(jnp.float32) for part in addends).astype(jnp.bfloat16)
-    return addends
+    wide = weight.shape[1] // CHUNKS
+    sums = []
+    for k in range(CHUNKS):
+        columns = weight[:, k * wide:(k + 1) * wide]
+        sent = dot32(sent_rows, columns).astype(jnp.bfloat16)
+        addends = [dot32(kept_rows, columns).astype(jnp.bfloat16)]
+        for bit in bits:
+            addends.append(across_ep(sent, 1 << bit))
+            rows = addends[-1].shape[0]
+            sent = sum(part[rows // 2:rows].astype(jnp.float32) for part in addends).astype(jnp.bfloat16)
+        sums += addends
+    return sums
 
 
 def dot32(left, right):
@@ -70,31 +76,25 @@
     return pl.multiple_of((CORES * place + (ids[1] ^ other)) * quarter, 128)
 
 
-def prepare_body(capacity, ids, routes, routes_t, prob, tokens, rate_param, chosen, combine, scale, decay):
-    rows, topk = routes.shape
+def prepare_body(capacity, ids, routes, prob, tokens, rate_param, chosen, combine, scale, decay):
+    topk, rows = routes.shape
     slots = chosen.shape[0]
     n_ep = slots // capacity
     down = lax.broadcasted_iota(jnp.int32, (rows, rows), 0)
     across = lax.broadcasted_iota(jnp.int32, (rows, rows), 1)
-    earlier = (across < down).astype(jnp.bfloat16)
-    earlier_t = (down < across).astype(jnp.bfloat16)
-    expert = lax.broadcasted_iota(jnp.int32, (rows, n_ep), 1)
-    expert_t = lax.broadcasted_iota(jnp.int32, (n_ep, rows), 0)
-    named = [(expert == routes[:, k:k + 1]).astype(jnp.float32) for k in range(topk)]
-    named_t = [(expert_t == routes_t[k:k + 1, :]).astype(jnp.float32) for k in range(topk)]
-    before = dot32(earlier, sum(named).astype(jnp.bfloat16))
-    before_t = dot32(sum(named_t).astype(jnp.bfloat16), earlier_t)
-    slot = lax.broadcasted_iota(jnp.int32, (rows, slots), 1)
-    slot_t = lax.broadcasted_iota(jnp.int32, (slots, rows), 0)
-    total = jnp.sum(prob[...], axis=1, keepdims=True)
+    earlier = (down < across).astype(jnp.bfloat16)
+    expert = lax.broadcasted_iota(jnp.int32, (n_ep, rows), 0)
+    named = [(expert == routes[k:k + 1, :]).astype(jnp.float32) for k in range(topk)]
+    before = dot32(sum(named).astype(jnp.bfloat16), earlier)
+    slot = lax.broadcasted_iota(jnp.int32, (slots, rows), 0)
+    total = jnp.sum(prob[...], axis=0, keepdims=True)
     picked, weighted = 0.0, 0.0
     for k in range(topk):
-        place = jnp.sum(before * named[k], axis=1, keepdims=True).astype(jnp.int32)
-        target = (routes[:, k:k + 1] ^ ids[0]) * capacity + place
-        weighted = weighted + jnp.where(slot == target, prob[:, k:k + 1] / total, 0.0)
-        place_t = jnp.sum(before_t * named_t[k], axis=0, keepdims=True).astype(jnp.int32)
-        target_t = (routes_t[k:k + 1, :] ^ ids[0]) * capacity + place_t
-        picked = picked + jnp.where(slot_t == target_t, 1.0, 0.0)
+        place = jnp.sum(before * named[k], axis=0, keepdims=True).astype(jnp.int32)
+        target = (routes[k:k + 1, :] ^ ids[0]) * capacity + place
+        picked = picked + jnp.where(slot == target, 1.0, 0.0)
+        weighted = weighted + jnp.where(slot == target, prob[k:k + 1, :] / total, 0.0)
+    weighted = weighted.T
     chosen[...] = picked.astype(jnp.bfloat16)
     high = weighted.astype(jnp.bfloat16)
     combine[:rows, :] = high
@@ -127,7 +127,14 @@
     rows = scale.shape[0]
     quarter = out_weight.shape[1] // n_tp
     row_scale = scale[...]
-    total = sum(part[:rows, :].astype(jnp.float32) for part in addends_x)
+    count = n_addends // CHUNKS
+    total = jnp.concatenate(
+        [
+            sum(part[:rows, :].astype(jnp.float32) for part in addends_x[k * count:(k + 1) * count])
+            for k in range(CHUNKS)
+        ],
+        axis=1,
+    )
     moved = (total * row_scale).astype(jnp.bfloat16)
     window_out[0] = history[1]
     window_out[1] = history[2]
@@ -149,7 +156,10 @@
         left = jnp.where(twice > -0.03, series, 1.0 - jnp.exp(twice))
         state = jnp.exp(log_decay) * state_in[:, at] + jnp.sqrt(left) * in_gate * part.astype(jnp.float32)
         state_out[:, at] = state
-        proj_y = sum(part[:rows, at].astype(jnp.float32) for part in addends_y) * row_scale
+        piece, inner = divmod(n * wide, addends_y[0].shape[1])
+        inner = slice(inner, inner + wide)
+        parts = addends_y[piece * count:(piece + 1) * count]
+        proj_y = sum(part[:rows, inner].astype(jnp.float32) for part in parts) * row_scale
         gated.append((state * jax.nn.gelu(proj_y, approximate=True)).astype(jnp.bfloat16))
     gated = jnp.concatenate(gated, axis=1)
     for other, target in ((1, send), (0, keep)):
@@ -159,43 +169,34 @@
             target[:, at] = dot32(gated, out_weight[:, columns]).astype(jnp.bfloat16)
 
 
-def merge_body(n_y, ids, tokens, first, second, mixed, squares):
+def dispatch_body(n_y, far, ids, tokens, first, second, gain, chosen, mixed, *refs):
+    sends, gained = refs[:-1], refs[-1]
     quarter = first.shape[1] // n_y
-    total = 0.0
     for place in range(n_y):
         at = slice(place * quarter, (place + 1) * quarter)
-        base = tokens[:, pl.ds(core_column(ids, place, 0, quarter), quarter)].astype(jnp.float32)
+        columns = pl.ds(core_column(ids, place, 0, quarter), quarter)
+        base = tokens[:, columns].astype(jnp.float32)
         part = base + (first[:, at].astype(jnp.float32) + second[:, at].astype(jnp.float32))
         mixed[:, at] = part
-        total = total + jnp.sum(part * part, axis=-1, keepdims=True)
-    squares[...] = total
-
-
-def dispatch_body(n_y, early, ids, mixed, squares, others, gain, chosen, *refs):
-    sends, normed = refs[:-1], refs[-1]
-    half = mixed.shape[1]
-    quarter = half // n_y
-    scale = lax.rsqrt((squares[...] + others[...]) / (CORES * half) + 1e-06)
-    for place in range(n_y):
-        at = slice(place * quarter, (place + 1) * quarter)
-        own_gain = gain[:, pl.ds(core_column(ids, place, 0, quarter), quarter)]
-        normed[:, at] = (mixed[:, at] * scale * own_gain).astype(jnp.bfloat16)
+        gained[:, at] = (part * gain[:, columns]).astype(jnp.bfloat16)
     capacity = sends[0].shape[0]
-    first = early[0] * capacity
-    rows = dot32(chosen[:first, :], normed[...]).astype(jnp.bfloat16)
-    for d in range(early[0]):
+    split = far * capacity
+    columns = pl.ds(pl.multiple_of(ids[2] * quarter, 128), quarter)
+    rows = dot32(chosen[split:, :], gained[:, columns]).astype(jnp.bfloat16)
+    for k in range(len(sends) - far):
+        sends[far + k][...] = rows[k * capacity:(k + 1) * capacity]
+    rows = dot32(chosen[:split, :], gained[...]).astype(jnp.bfloat16)
+    for d in range(far):
         sends[d][...] = rows[d * capacity:(d + 1) * capacity]
-    columns = pl.ds(pl.multiple_of(ids[2] * quarter, 128), quarter)
-    rows = dot32(chosen[first:, :], normed[:, columns]).astype(jnp.bfloat16)
-    for k, d in enumerate(early):
-        sends[d][...] = rows[k * capacity:(k + 1) * capacity]
 
 
 def expert_body(n_tp, n_pieces, swapped, ids, *refs):
-    pieces, (gate, up, down, keep, send) = refs[:CORES * n_pieces], refs[CORES * n_pieces:]
+    pieces, (gain, gate, up, down, keep, send) = refs[:CORES * n_pieces], refs[CORES * n_pieces:]
     quarter = gate.shape[1] // n_tp
     n_y = n_tp // CORES
-    gate_part, up_part = None, None
+    slots = keep.shape[0]
+    copies = 2 if slots < 128 else 1
+    gate_part, up_part, squares = None, None, 0.0
     for other in range(CORES):
         for place in range(n_y):
             if n_pieces == 1:
@@ -204,16 +205,22 @@
                 part = pieces[other * n_pieces + place][...]
             which = (ids[2] ^ place) if swapped else place
             span = pl.ds(core_column(ids, which, other, quarter), quarter)
+            plain = part.astype(jnp.float32) * (1.0 / gain[:, span])
+            squares = squares + jnp.sum(plain * plain, axis=-1, keepdims=True)
+            part = jnp.concatenate([part] * copies, axis=0)
             term = dot32(part, gate[0, span, :])
             gate_part = term if gate_part is None else gate_part + term
             term = dot32(part, up[0, span, :])
             up_part = term if up_part is None else up_part + term
+    scale = lax.rsqrt(squares / gate.shape[1] + 1e-06)
+    scale = jnp.concatenate([scale] * copies, axis=0)
+    gate_part, up_part = gate_part * scale, up_part * scale
     hidden = (jax.nn.silu(gate_part) * up_part).astype(jnp.bfloat16)
     for other, target in ((1, send), (0, keep)):
         for place in range(n_y):
             span = pl.ds(core_column(ids, ids[2] ^ place, other, quarter), quarter)
             at = slice(place * quarter, (place + 1) * quarter)
-            target[:, at] = dot32(hidden, down[0, :, span]).astype(jnp.bfloat16)
+            target[:, at] = dot32(hidden, down[0, :, span])[:slots].astype(jnp.bfloat16)
 
 
 def finish_body(ids, returned, mixed, combine, layer):
@@ -264,7 +271,7 @@
     theirs = across_cores(jnp.concatenate(mine, axis=0))
     chosen, combine, scale, decay = call(
         functools.partial(prepare_body, capacity), ids,
-        [routes, routes.T, route_prob, tokens, rate_param[None, :]],
+        [routes.T, route_prob.T, tokens, rate_param[None, :]],
         [((slots, rows), bf16), ((2 * rows, slots), bf16), ((rows, 1), f32), ((1, channels), f32)],
         8,
     )
@@ -299,24 +306,20 @@
         first = (first.astype(f32) + second.astype(f32)).astype(bf16)
         second = across_y(first, offset)
         offset *= 2
-    mixed, squares = call(
-        functools.partial(merge_body, n_y), ids, [tokens, first, second],
-        [((rows, half), f32), ((rows, 1), f32)], 8,
-    )
     near = list(range(n_ep // 2))
     early = list(range(3 * n_ep // 4, n_ep))
     late = list(range(n_ep // 2, 3 * n_ep // 4))
-    sends = pl.pallas_call(
-        functools.partial(dispatch_body, n_y, early),
+    second_gain = moe_gain[None, :].astype(f32)
+    mixed, *sends = pl.pallas_call(
+        functools.partial(dispatch_body, n_y, len(near)),
         in_specs=[pl.BlockSpec(memory_space=pltpu.SMEM)] + [pl.BlockSpec(memory_space=pltpu.VMEM)] * 5,
-        out_specs=[pl.BlockSpec(memory_space=pltpu.VMEM)] * n_ep,
-        out_shape=[
-            jax.ShapeDtypeStruct((capacity, quarter if d in early else half), bf16) for d in range(n_ep)
-        ],
+        out_specs=[pl.BlockSpec(memory_space=pltpu.VMEM)] * (1 + n_ep),
+        out_shape=[jax.ShapeDtypeStruct((rows, half), f32)]
+        + [jax.ShapeDtypeStruct((capacity, half if d in near else quarter), bf16) for d in range(n_ep)],
         scratch_shapes=[pltpu.VMEM((rows, half), bf16)],
         compiler_params=pltpu.CompilerParams(vmem_limit_bytes=8 << 20),
         name="dispatch",
-    )(ids, mixed, squares, across_cores(squares), moe_gain[None, :].astype(f32), chosen)
+    )(ids, tokens, first, second, second_gain, chosen)
 
     landed = {0: sends[0]}
     for group in (early, near[1:], late):
@@ -325,13 +328,13 @@
     back = {}
     for name, group in (("near", near), ("early", early), ("late", late)):
         pieces = [jnp.concatenate([landed[d] for d in group], axis=0)]
-        if name == "early":
+        if name != "near":
             pieces += [across_y(pieces[0], k) for k in range(1, n_y)]
         others = [across_cores(piece) for piece in pieces]
         count = len(group) * capacity
         keep, send = call(
-            functools.partial(expert_body, n_tp, len(pieces), name == "early"), ids,
-            [*pieces, *others, expert_gate, expert_up, expert_down], [((count, half), bf16)] * 2,
+            functools.partial(expert_body, n_tp, len(pieces), name != "near"), ids,
+            [*pieces, *others, second_gain, expert_gate, expert_up, expert_down], [((count, half), bf16)] * 2,
             20,
             cost_estimate=pl.CostEstimate(
                 flops=6 * count * width * expert_gate.shape[2], bytes_accessed=0, transcendentals=0

time: 144 us -> 131 us (0.910)
  local copies, waits for them, and re-layouts: 16.4 us -> 2.08 us
  starting transfers between devices: 43.7 us -> 49.9 us
  waiting for transfers between devices: 60.8 us -> 58.5 us
  Pallas kernels: 16.9 us -> 15 us
  matrix products: 1.78 us -> 3.56 us
    unnamed x57 -> x45, local copies, waits for them, and re-layouts: 14.5 us -> 0.19 us
    ppermute x39 -> x46, starting transfers between devices: 43.7 us -> 49.9 us  [send_to(): return lax.ppermute(value, AXES, pairs)]
    ppermute x39 -> x46, waiting for transfers between devices: 60.8 us -> 58.5 us  [send_to(): return lax.ppermute(value, AXES, pairs)]
    pallas_call x8 -> x7, Pallas kernels: 15.9 us -> 14 us  [call(): pl.pallas_call(body, in_specs=[pl.BlockSpec(memory_space=pltpu.SMEM)] + [...]
    dot_general x4 -> x8, matrix products: 1.78 us -> 3.56 us  [dot32(): return jnp.dot(left, right, preferred_element_type=jnp.float32)]
  transfers between devices with their start and end apart: 39 -> 46, of which waited for: 20 -> 25; matrix products, arithmetic and copies ran while one was open for 5% -> 2% of each run, Pallas kernels for 6% -> 6%
where the time goes in v2:
time: 131 us
  waiting for transfers between devices  58.5 us (45%)
  starting transfers between devices  49.9 us (38%)
  Pallas kernels  15 us (11%)
  matrix products  3.56 us (3%)
  local copies, waits for them, and re-layouts  2.08 us (2%)
    ppermute x46, waiting for transfers between devices, send_to(): return lax.ppermute(value, AXES, pairs)  58.5 us
    ppermute x46, starting transfers between devices, send_to(): return lax.ppermute(value, AXES, pairs)  49.9 us
    pallas_call x7, Pallas kernels, call(): pl.pallas_call(body, in_specs=[pl.BlockSpec(memory_space=pltpu.SMEM)] + [...  14 us
    dot_general x8, matrix products, dot32(): return jnp.dot(left, right, preferred_element_type=jnp.float32)  3.56 us
  transfers between devices with their start and end apart: 46, of which 25 were waited for; matrix products, arithmetic and copies ran while one was open for 2% of the time, Pallas kernels for 6%

profile of v2, /device:TPU:0, one launch (start us, length us, event | category | flops | bytes accessed | tf_op | source)
XLA Modules:
  0.0 131.1 jit_solution(4999023135618530479)
XLA Ops:
  2.4 3.1 %collective-permute-start.1 = (bf16[64,512]{1,0:T(8,128)(2,1)S(1)}, bf16[64,512]{1,0:T(8,128)(2,1)S(1)}, u32[]{:S(2)}, u32[]{:S(2)}) collective-permute-start(bf16[64,512]{1,0:T(8,128)(2,1)S(1)} %get-tuple-element.55), channel_id=1, source_target_pairs={{0,8},{1,13},{2,10},{3,15},{4,12},{5,9},{6,14},{7,11},{8,0},{9,5},... | collective-permute-start | bytes 196616 | tf_op jit(solution)/shard_map/ppermute | solution.py:23
  5.5 2.6 %collective-permute-start.2 = (bf16[64,512]{1,0:T(8,128)(2,1)S(1)}, bf16[64,512]{1,0:T(8,128)(2,1)S(1)}, u32[]{:S(2)}, u32[]{:S(2)}) collective-permute-start(bf16[64,512]{1,0:T(8,128)(2,1)S(1)} %get-tuple-element.54), channel_id=1, source_target_pairs={{0,16},{1,21},{2,18},{3,23},{4,20},{5,17},{6,22},{7,19},{8,24},{9,... | collective-permute-start | bytes 196616 | tf_op jit(solution)/shard_map/ppermute | solution.py:23
  8.1 3.3 %collective-permute-done.2.refs_2_ = bf16[64,512]{1,0:T(8,128)(2,1)S(1)} collective-permute-done((bf16[64,512]{1,0:T(8,128)(2,1)S(1)}, bf16[64,512]{1,0:T(8,128)(2,1)S(1)}, u32[]{:S(2)}, u32[]{:S(2)}) %collective-permute-start.2) | collective-permute-done | bytes 65568 | tf_op jit(solution)/shard_map/ppermute | solution.py:23
  11.4 2.9 %collective-permute-done.3.refs_3_ = bf16[64,512]{1,0:T(8,128)(2,1)S(1)} collective-permute-done((bf16[64,512]{1,0:T(8,128)(2,1)S(1)}, bf16[64,512]{1,0:T(8,128)(2,1)S(1)}, u32[]{:S(2)}, u32[]{:S(2)}) %collective-permute-start.3) | collective-permute-done | bytes 65568 | tf_op jit(solution)/shard_map/ppermute | solution.py:23
  14.3 2.3 %collective-permute-start.4 = (bf16[256,512]{1,0:T(8,128)(2,1)S(1)}, bf16[256,512]{1,0:T(8,128)(2,1)S(1)}, u32[]{:S(2)}, u32[]{:S(2)}) collective-permute-start(bf16[256,512]{1,0:T(8,128)(2,1)S(1)} %pad_maximum_fusion.4), channel_id=1, source_target_pairs={{0,1},{1,0},{2,3},{3,2},{4,5},{5,4},{6,7},{7,6},{8,9},{9,8},{10,11... | collective-permute-start | bytes 786440 | tf_op jit(solution)/shard_map/ppermute | solution.py:23
  26.5 4.4 %collective-permute-done.14.refs_13_ = bf16[256,512]{1,0:T(8,128)(2,1)S(1)} collective-permute-done((bf16[256,512]{1,0:T(8,128)(2,1)S(1)}, bf16[256,512]{1,0:T(8,128)(2,1)S(1)}, u32[]{:S(2)}, u32[]{:S(2)}) %collective-permute-start.14) | collective-permute-done | bytes 262176 | tf_op jit(solution)/shard_map/ppermute | solution.py:23
  31.5 4.4 %collective-permute-done.11.refs_9_ = bf16[256,512]{1,0:T(8,128)(2,1)S(1)} collective-permute-done((bf16[256,512]{1,0:T(8,128)(2,1)S(1)}, bf16[256,512]{1,0:T(8,128)(2,1)S(1)}, u32[]{:S(2)}, u32[]{:S(2)}) %collective-permute-start.11) | collective-permute-done | bytes 262176 | tf_op jit(solution)/shard_map/ppermute | solution.py:23
  36.9 2.3 %collective-permute-done.5.refs_1_ = bf16[256,512]{1,0:T(8,128)(2,1)S(1)} collective-permute-done((bf16[256,512]{1,0:T(8,128)(2,1)S(1)}, bf16[256,512]{1,0:T(8,128)(2,1)S(1)}, u32[]{:S(2)}, u32[]{:S(2)}) %collective-permute-start.5) | collective-permute-done | bytes 262176 | tf_op jit(solution)/shard_map/ppermute | solution.py:23
  39.4 2.7 %collective-permute-done.15.refs_14_ = bf16[128,512]{1,0:T(8,128)(2,1)S(1)} collective-permute-done((bf16[128,512]{1,0:T(8,128)(2,1)S(1)}, bf16[128,512]{1,0:T(8,128)(2,1)S(1)}, u32[]{:S(2)}, u32[]{:S(2)}) %collective-permute-start.15) | collective-permute-done | bytes 131104 | tf_op jit(solution)/shard_map/ppermute | solution.py:23
  49.1 3.3 %collective-permute-done.16.refs_15_ = bf16[64,512]{1,0:T(8,128)(2,1)S(1)} collective-permute-done((bf16[64,512]{1,0:T(8,128)(2,1)S(1)}, bf16[64,512]{1,0:T(8,128)(2,1)S(1)}, u32[]{:S(2)}, u32[]{:S(2)}) %collective-permute-start.16) | collective-permute-done | bytes 65568 | tf_op jit(solution)/shard_map/ppermute | solution.py:23
  56.0 3.4 %shard_map.186 = (f32[64,1024]{1,0:T(8,128)}, bf16[3,64,1024]{2,1,0:T(8,128)(2,1)}, bf16[64,2048]{1,0:T(8,128)(2,1)S(1)}, bf16[64,2048]{1,0:T(8,128)(2,1)S(1)}) custom-call(s32[3]{0:T(128)S(1)} %add_convert_fusion.15.ids, bf16[256,512]{1,0:T(8,128)(2,1)S(1)} %convolution_convert_fusion.7.refs_0_, bf16[256,512]{1,0:T(8,128)(2,1)S(1)} %collective-permute-done.5.refs_1_, ...), custom_call_target="tpu_custom_call" | custom-call | tf_op jit(solution)/shard_map/pallas_call | solution.py:65
  62.6 6.8 %collective-permute-done.18.second = bf16[64,2048]{1,0:T(8,128)(2,1)S(1)} collective-permute-done((bf16[64,2048]{1,0:T(8,128)(2,1)S(1)}, bf16[64,2048]{1,0:T(8,128)(2,1)S(1)}, u32[]{:S(2)}, u32[]{:S(2)}) %collective-permute-start.18) | collective-permute-done | bytes 262176 | tf_op jit(solution)/shard_map/ppermute | solution.py:23
  72.4 2.2 %collective-permute-start.38 = (bf16[32,1024]{1,0:T(8,128)(2,1)S(1)}, bf16[32,1024]{1,0:T(8,128)(2,1)S(1)}, u32[]{:S(2)}, u32[]{:S(2)}) collective-permute-start(bf16[32,1024]{1,0:T(8,128)(2,1)S(1)} %get-tuple-element.46), channel_id=1, source_target_pairs={{0,28},{1,29},{2,30},{3,31},{4,24},{5,25},{6,26},{7,27},{8,20},{9,... | collective-permute-start | bytes 196616 | tf_op jit(solution)/shard_map/ppermute | solution.py:23
  74.6 3.7 %collective-permute-start.29 = (bf16[32,1024]{1,0:T(8,128)(2,1)S(1)}, bf16[32,1024]{1,0:T(8,128)(2,1)S(1)}, u32[]{:S(2)}, u32[]{:S(2)}) collective-permute-start(bf16[32,1024]{1,0:T(8,128)(2,1)S(1)} %get-tuple-element.42), channel_id=1, source_target_pairs={{0,20},{1,21},{2,22},{3,23},{4,16},{5,17},{6,18},{7,19},{8,28},{9,... | collective-permute-start | bytes 196616 | tf_op jit(solution)/shard_map/ppermute | solution.py:23
  79.6 2.3 %collective-permute-start.21 = (bf16[32,2048]{1,0:T(8,128)(2,1)S(1)}, bf16[32,2048]{1,0:T(8,128)(2,1)S(1)}, u32[]{:S(2)}, u32[]{:S(2)}) collective-permute-start(bf16[32,2048]{1,0:T(8,128)(2,1)S(1)} %get-tuple-element.38), channel_id=1, source_target_pairs={{0,12},{1,13},{2,14},{3,15},{4,8},{5,9},{6,10},{7,11},{8,4},{9,5},... | collective-permute-start | bytes 393224 | tf_op jit(solution)/shard_map/ppermute | solution.py:23
  87.0 3.0 %collective-permute-done.30.refs_1_ = bf16[64,1024]{1,0:T(8,128)(2,1)S(1)} collective-permute-done((bf16[64,1024]{1,0:T(8,128)(2,1)S(1)}, bf16[64,1024]{1,0:T(8,128)(2,1)S(1)}, u32[]{:S(2)}, u32[]{:S(2)}) %collective-permute-start.30) | collective-permute-done | bytes 131104 | tf_op jit(solution)/shard_map/ppermute | solution.py:23
  90.0 2.5 %shard_map.189 = (bf16[64,2048]{1,0:T(8,128)(2,1)S(1)}, bf16[64,2048]{1,0:T(8,128)(2,1)S(1)}) custom-call(s32[3]{0:T(128)S(1)} %add_convert_fusion.15.ids, bf16[64,1024]{1,0:T(8,128)(2,1)S(1)} %constant_dynamic-update-slice_fusion.6.refs_0_, bf16[64,1024]{1,0:T(8,128)(2,1)S(1)} %collective-permute-done.39.refs_1_, ...), custom_call_target="tpu_custom_call" | custom-call | flops 805306368 | tf_op jit(solution)/shard_map/pallas_call | solution.py:65
  93.2 2.5 %shard_map.188 = (bf16[64,2048]{1,0:T(8,128)(2,1)S(1)}, bf16[64,2048]{1,0:T(8,128)(2,1)S(1)}) custom-call(s32[3]{0:T(128)S(1)} %add_convert_fusion.15.ids, bf16[64,1024]{1,0:T(8,128)(2,1)S(1)} %constant_dynamic-update-slice_fusion.4.refs_0_, bf16[64,1024]{1,0:T(8,128)(2,1)S(1)} %collective-permute-done.30.refs_1_, ...), custom_call_target="tpu_custom_call" | custom-call | flops 805306368 | tf_op jit(solution)/shard_map/pallas_call | solution.py:65
  98.0 2.6 %shard_map.187 = (bf16[128,2048]{1,0:T(8,128)(2,1)S(1)}, bf16[128,2048]{1,0:T(8,128)(2,1)S(1)}) custom-call(s32[3]{0:T(128)S(1)} %add_convert_fusion.15.ids, bf16[128,2048]{1,0:T(8,128)(2,1)S(1)} %constant_dynamic-update-slice_fusion.refs_0_, bf16[128,2048]{1,0:T(8,128)(2,1)S(1)} %collective-permute-done.22.refs_1_, f32[1,4096]{1,0:T(1,128)S(1)} %bitcast.14, ...), custom_call_target="tpu_custom_call" | custom-call | flops 1610612736 | tf_op jit(solution)/shard_map/pallas_call | solution.py:65
  107.3 5.1 %collective-permute-done.24 = bf16[128,1024]{1,0:T(8,128)(2,1)S(1)} collective-permute-done((bf16[128,1024]{1,0:T(8,128)(2,1)S(1)}, bf16[128,1024]{1,0:T(8,128)(2,1)S(1)}, u32[]{:S(2)}, u32[]{:S(2)}) %collective-permute-start.24) | collective-permute-done | bytes 262176 | tf_op jit(solution)/shard_map/ppermute | solution.py:23
  114.2 2.8 %collective-permute-start.36 = (bf16[32,1024]{1,0:T(8,128)(2,1)S(1)}, bf16[32,1024]{1,0:T(8,128)(2,1)S(1)}, u32[]{:S(2)}, u32[]{:S(2)}) collective-permute-start(bf16[32,1024]{1,0:T(8,128)(2,1)S(1)} %get-tuple-element.71), channel_id=1, source_target_pairs={{0,20},{1,21},{2,22},{3,23},{4,16},{5,17},{6,18},{7,19},{8,28},{9,... | collective-permute-start | bytes 196616 | tf_op jit(solution)/shard_map/ppermute | solution.py:23
  117.0 2.6 %collective-permute-start.45 = (bf16[32,1024]{1,0:T(8,128)(2,1)S(1)}, bf16[32,1024]{1,0:T(8,128)(2,1)S(1)}, u32[]{:S(2)}, u32[]{:S(2)}) collective-permute-start(bf16[32,1024]{1,0:T(8,128)(2,1)S(1)} %get-tuple-element.69), channel_id=1, source_target_pairs={{0,28},{1,29},{2,30},{3,31},{4,24},{5,25},{6,26},{7,27},{8,20},{9,... | collective-permute-start | bytes 196616 | tf_op jit(solution)/shard_map/ppermute | solution.py:23
  119.6 4.8 %collective-permute-done.26 = bf16[32,1024]{1,0:T(8,128)(2,1)S(1)} collective-permute-done((bf16[32,1024]{1,0:T(8,128)(2,1)S(1)}, bf16[32,1024]{1,0:T(8,128)(2,1)S(1)}, u32[]{:S(2)}, u32[]{:S(2)}) %collective-permute-start.26) | collective-permute-done | bytes 65568 | tf_op jit(solution)/shard_map/ppermute | solution.py:23
  124.8 4.8 %collective-permute-done.27 = bf16[32,1024]{1,0:T(8,128)(2,1)S(1)} collective-permute-done((bf16[32,1024]{1,0:T(8,128)(2,1)S(1)}, bf16[32,1024]{1,0:T(8,128)(2,1)S(1)}, u32[]{:S(2)}, u32[]{:S(2)}) %collective-permute-start.27) | collective-permute-done | bytes 65568 | tf_op jit(solution)/shard_map/ppermute | solution.py:23
  (161 shorter events, 49.3 us)
Async XLA Ops:
  21.6 9.2 %collective-permute-start.14 = (bf16[256,512]{1,0:T(8,128)(2,1)S(1)}, bf16[256,512]{1,0:T(8,128)(2,1)S(1)}, u32[]{:S(2)}, u32[]{:S(2)}) collective-permute-start(bf16[256,512]{1,0:T(8,128)(2,1)S(1)} %convolution_convert_fusion), channel_id=1, source_target_pairs={{0,8},{1,9},{2,10},{3,11},{4,12},{5,13},{6,14},{7,15},{8,0},{9,1},... | collective-permute-start | bytes 786440 | tf_op jit(solution)/shard_map/ppermute | solution.py:23
  22.0 13.9 %collective-permute-start.11 = (bf16[256,512]{1,0:T(8,128)(2,1)S(1)}, bf16[256,512]{1,0:T(8,128)(2,1)S(1)}, u32[]{:S(2)}, u32[]{:S(2)}) collective-permute-start(bf16[256,512]{1,0:T(8,128)(2,1)S(1)} %convolution_convert_fusion.2), channel_id=1, source_target_pairs={{0,8},{1,9},{2,10},{3,11},{4,12},{5,13},{6,14},{7,15},{8,0},{9,1},... | collective-permute-start | bytes 786440 | tf_op jit(solution)/shard_map/ppermute | solution.py:23
  24.4 12.1 %collective-permute-start.8 = (bf16[256,512]{1,0:T(8,128)(2,1)S(1)}, bf16[256,512]{1,0:T(8,128)(2,1)S(1)}, u32[]{:S(2)}, u32[]{:S(2)}) collective-permute-start(bf16[256,512]{1,0:T(8,128)(2,1)S(1)} %convolution_convert_fusion.4), channel_id=1, source_target_pairs={{0,4},{1,5},{2,6},{3,7},{4,0},{5,1},{6,2},{7,3},{8,12},{9,13},{10,... | collective-permute-start | bytes 786440 | tf_op jit(solution)/shard_map/ppermute | solution.py:23
  25.0 14.3 %collective-permute-start.5 = (bf16[256,512]{1,0:T(8,128)(2,1)S(1)}, bf16[256,512]{1,0:T(8,128)(2,1)S(1)}, u32[]{:S(2)}, u32[]{:S(2)}) collective-permute-start(bf16[256,512]{1,0:T(8,128)(2,1)S(1)} %convolution_convert_fusion.6), channel_id=1, source_target_pairs={{0,4},{1,5},{2,6},{3,7},{4,0},{5,1},{6,2},{7,3},{8,12},{9,13},{10,... | collective-permute-start | bytes 786440 | tf_op jit(solution)/shard_map/ppermute | solution.py:23
  30.9 11.2 %collective-permute-start.15 = (bf16[128,512]{1,0:T(8,128)(2,1)S(1)}, bf16[128,512]{1,0:T(8,128)(2,1)S(1)}, u32[]{:S(2)}, u32[]{:S(2)}) collective-permute-start(bf16[128,512]{1,0:T(8,128)(2,1)S(1)} %add_convert_fusion.7), channel_id=1, source_target_pairs={{0,4},{1,5},{2,6},{3,7},{4,0},{5,1},{6,2},{7,3},{8,12},{9,13},{10,... | collective-permute-start | bytes 393224 | tf_op jit(solution)/shard_map/ppermute | solution.py:23
  35.9 7.8 %collective-permute-start.12 = (bf16[128,512]{1,0:T(8,128)(2,1)S(1)}, bf16[128,512]{1,0:T(8,128)(2,1)S(1)}, u32[]{:S(2)}, u32[]{:S(2)}) collective-permute-start(bf16[128,512]{1,0:T(8,128)(2,1)S(1)} %add_convert_fusion.8), channel_id=1, source_target_pairs={{0,4},{1,5},{2,6},{3,7},{4,0},{5,1},{6,2},{7,3},{8,12},{9,13},{10,... | collective-permute-start | bytes 393224 | tf_op jit(solution)/shard_map/ppermute | solution.py:23
  36.6 8.6 %collective-permute-start.9 = (bf16[128,512]{1,0:T(8,128)(2,1)S(1)}, bf16[128,512]{1,0:T(8,128)(2,1)S(1)}, u32[]{:S(2)}, u32[]{:S(2)}) collective-permute-start(bf16[128,512]{1,0:T(8,128)(2,1)S(1)} %add_convert_fusion.9), channel_id=1, source_target_pairs={{0,8},{1,9},{2,10},{3,11},{4,12},{5,13},{6,14},{7,15},{8,0},{9,1},... | collective-permute-start | bytes 393224 | tf_op jit(solution)/shard_map/ppermute | solution.py:23
  39.3 7.5 %collective-permute-start.6 = (bf16[128,512]{1,0:T(8,128)(2,1)S(1)}, bf16[128,512]{1,0:T(8,128)(2,1)S(1)}, u32[]{:S(2)}, u32[]{:S(2)}) collective-permute-start(bf16[128,512]{1,0:T(8,128)(2,1)S(1)} %add_convert_fusion.10), channel_id=1, source_target_pairs={{0,8},{1,9},{2,10},{3,11},{4,12},{5,13},{6,14},{7,15},{8,0},{9,1},... | collective-permute-start | bytes 393224 | tf_op jit(solution)/shard_map/ppermute | solution.py:23
  42.1 10.3 %collective-permute-start.16 = (bf16[64,512]{1,0:T(8,128)(2,1)S(1)}, bf16[64,512]{1,0:T(8,128)(2,1)S(1)}, u32[]{:S(2)}, u32[]{:S(2)}) collective-permute-start(bf16[64,512]{1,0:T(8,128)(2,1)S(1)} %add_convert_fusion.11), channel_id=1, source_target_pairs={{0,16},{1,17},{2,18},{3,19},{4,20},{5,21},{6,22},{7,23},{8,24},{9,... | collective-permute-start | bytes 196616 | tf_op jit(solution)/shard_map/ppermute | solution.py:23
  43.8 10.1 %collective-permute-start.13 = (bf16[64,512]{1,0:T(8,128)(2,1)S(1)}, bf16[64,512]{1,0:T(8,128)(2,1)S(1)}, u32[]{:S(2)}, u32[]{:S(2)}) collective-permute-start(bf16[64,512]{1,0:T(8,128)(2,1)S(1)} %add_convert_fusion.12), channel_id=1, source_target_pairs={{0,16},{1,17},{2,18},{3,19},{4,20},{5,21},{6,22},{7,23},{8,24},{9,... | collective-permute-start | bytes 196616 | tf_op jit(solution)/shard_map/ppermute | solution.py:23
  45.2 10.0 %collective-permute-start.10 = (bf16[64,512]{1,0:T(8,128)(2,1)S(1)}, bf16[64,512]{1,0:T(8,128)(2,1)S(1)}, u32[]{:S(2)}, u32[]{:S(2)}) collective-permute-start(bf16[64,512]{1,0:T(8,128)(2,1)S(1)} %add_convert_fusion.13), channel_id=1, source_target_pairs={{0,16},{1,17},{2,18},{3,19},{4,20},{5,21},{6,22},{7,23},{8,24},{9,... | collective-permute-start | bytes 196616 | tf_op jit(solution)/shard_map/ppermute | solution.py:23
  46.9 9.0 %collective-permute-start.7 = (bf16[64,512]{1,0:T(8,128)(2,1)S(1)}, bf16[64,512]{1,0:T(8,128)(2,1)S(1)}, u32[]{:S(2)}, u32[]{:S(2)}) collective-permute-start(bf16[64,512]{1,0:T(8,128)(2,1)S(1)} %add_convert_fusion.14), channel_id=1, source_target_pairs={{0,16},{1,17},{2,18},{3,19},{4,20},{5,21},{6,22},{7,23},{8,24},{9,... | collective-permute-start | bytes 196616 | tf_op jit(solution)/shard_map/ppermute | solution.py:23
  61.1 8.4 %collective-permute-start.18 = (bf16[64,2048]{1,0:T(8,128)(2,1)S(1)}, bf16[64,2048]{1,0:T(8,128)(2,1)S(1)}, u32[]{:S(2)}, u32[]{:S(2)}) collective-permute-start(bf16[64,2048]{1,0:T(8,128)(2,1)S(1)} %add_convert_fusion.4.first), channel_id=1, source_target_pairs={{0,2},{1,3},{2,0},{3,1},{4,6},{5,7},{6,4},{7,5},{8,10},{9,11},{10,... | collective-permute-start | bytes 786440 | tf_op jit(solution)/shard_map/ppermute | solution.py:23
  70.5 8.5 %collective-permute-start.37 = (bf16[32,1024]{1,0:T(8,128)(2,1)S(1)}, bf16[32,1024]{1,0:T(8,128)(2,1)S(1)}, u32[]{:S(2)}, u32[]{:S(2)}) collective-permute-start(bf16[32,1024]{1,0:T(8,128)(2,1)S(1)} %get-tuple-element.45), channel_id=1, source_target_pairs={{0,24},{1,25},{2,26},{3,27},{4,28},{5,29},{6,30},{7,31},{8,16},{9,... | collective-permute-start | bytes 196616 | tf_op jit(solution)/shard_map/ppermute | solution.py:23
  72.4 7.3 %collective-permute-start.38 = (bf16[32,1024]{1,0:T(8,128)(2,1)S(1)}, bf16[32,1024]{1,0:T(8,128)(2,1)S(1)}, u32[]{:S(2)}, u32[]{:S(2)}) collective-permute-start(bf16[32,1024]{1,0:T(8,128)(2,1)S(1)} %get-tuple-element.46), channel_id=1, source_target_pairs={{0,28},{1,29},{2,30},{3,31},{4,24},{5,25},{6,26},{7,27},{8,20},{9,... | collective-permute-start | bytes 196616 | tf_op jit(solution)/shard_map/ppermute | solution.py:23
  74.6 7.3 %collective-permute-start.28 = (bf16[32,1024]{1,0:T(8,128)(2,1)S(1)}, bf16[32,1024]{1,0:T(8,128)(2,1)S(1)}, u32[]{:S(2)}, u32[]{:S(2)}) collective-permute-start(bf16[32,1024]{1,0:T(8,128)(2,1)S(1)} %get-tuple-element.41), channel_id=1, source_target_pairs={{0,16},{1,17},{2,18},{3,19},{4,20},{5,21},{6,22},{7,23},{8,24},{9,... | collective-permute-start | bytes 196616 | tf_op jit(solution)/shard_map/ppermute | solution.py:23
  74.6 9.4 %collective-permute-start.29 = (bf16[32,1024]{1,0:T(8,128)(2,1)S(1)}, bf16[32,1024]{1,0:T(8,128)(2,1)S(1)}, u32[]{:S(2)}, u32[]{:S(2)}) collective-permute-start(bf16[32,1024]{1,0:T(8,128)(2,1)S(1)} %get-tuple-element.42), channel_id=1, source_target_pairs={{0,20},{1,21},{2,22},{3,23},{4,16},{5,17},{6,18},{7,19},{8,28},{9,... | collective-permute-start | bytes 196616 | tf_op jit(solution)/shard_map/ppermute | solution.py:23
  79.0 7.2 %collective-permute-start.20 = (bf16[32,2048]{1,0:T(8,128)(2,1)S(1)}, bf16[32,2048]{1,0:T(8,128)(2,1)S(1)}, u32[]{:S(2)}, u32[]{:S(2)}) collective-permute-start(bf16[32,2048]{1,0:T(8,128)(2,1)S(1)} %get-tuple-element.37), channel_id=1, source_target_pairs={{0,8},{1,9},{2,10},{3,11},{4,12},{5,13},{6,14},{7,15},{8,0},{9,1},... | collective-permute-start | bytes 393224 | tf_op jit(solution)/shard_map/ppermute | solution.py:23
  79.6 13.4 %collective-permute-start.21 = (bf16[32,2048]{1,0:T(8,128)(2,1)S(1)}, bf16[32,2048]{1,0:T(8,128)(2,1)S(1)}, u32[]{:S(2)}, u32[]{:S(2)}) collective-permute-start(bf16[32,2048]{1,0:T(8,128)(2,1)S(1)} %get-tuple-element.38), channel_id=1, source_target_pairs={{0,12},{1,13},{2,14},{3,15},{4,8},{5,9},{6,10},{7,11},{8,4},{9,5},... | collective-permute-start | bytes 393224 | tf_op jit(solution)/shard_map/ppermute | solution.py:23
  102.7 9.6 %collective-permute-start.24 = (bf16[128,1024]{1,0:T(8,128)(2,1)S(1)}, bf16[128,1024]{1,0:T(8,128)(2,1)S(1)}, u32[]{:S(2)}, u32[]{:S(2)}) collective-permute-start(bf16[128,1024]{1,0:T(8,128)(2,1)S(1)} %slice.205), channel_id=1, source_target_pairs={{0,2},{1,3},{2,0},{3,1},{4,6},{5,7},{6,4},{7,5},{8,10},{9,11},{10,... | collective-permute-start | bytes 786440 | tf_op jit(solution)/shard_map/ppermute | solution.py:23
  103.7 25.9 %collective-permute-start.44 = (bf16[32,1024]{1,0:T(8,128)(2,1)S(1)}, bf16[32,1024]{1,0:T(8,128)(2,1)S(1)}, u32[]{:S(2)}, u32[]{:S(2)}) collective-permute-start(bf16[32,1024]{1,0:T(8,128)(2,1)S(1)} %get-tuple-element.70), channel_id=1, source_target_pairs={{0,24},{1,25},{2,26},{3,27},{4,28},{5,29},{6,30},{7,31},{8,16},{9,... | collective-permute-start | bytes 196616 | tf_op jit(solution)/shard_map/ppermute | solution.py:23
  113.7 15.9 %collective-permute-start.35 = (bf16[32,1024]{1,0:T(8,128)(2,1)S(1)}, bf16[32,1024]{1,0:T(8,128)(2,1)S(1)}, u32[]{:S(2)}, u32[]{:S(2)}) collective-permute-start(bf16[32,1024]{1,0:T(8,128)(2,1)S(1)} %get-tuple-element.72), channel_id=1, source_target_pairs={{0,16},{1,17},{2,18},{3,19},{4,20},{5,21},{6,22},{7,23},{8,24},{9,... | collective-permute-start | bytes 196616 | tf_op jit(solution)/shard_map/ppermute | solution.py:23
  114.2 15.5 %collective-permute-start.36 = (bf16[32,1024]{1,0:T(8,128)(2,1)S(1)}, bf16[32,1024]{1,0:T(8,128)(2,1)S(1)}, u32[]{:S(2)}, u32[]{:S(2)}) collective-permute-start(bf16[32,1024]{1,0:T(8,128)(2,1)S(1)} %get-tuple-element.71), channel_id=1, source_target_pairs={{0,20},{1,21},{2,22},{3,23},{4,16},{5,17},{6,18},{7,19},{8,28},{9,... | collective-permute-start | bytes 196616 | tf_op jit(solution)/shard_map/ppermute | solution.py:23
  117.0 12.7 %collective-permute-start.45 = (bf16[32,1024]{1,0:T(8,128)(2,1)S(1)}, bf16[32,1024]{1,0:T(8,128)(2,1)S(1)}, u32[]{:S(2)}, u32[]{:S(2)}) collective-permute-start(bf16[32,1024]{1,0:T(8,128)(2,1)S(1)} %get-tuple-element.69), channel_id=1, source_target_pairs={{0,28},{1,29},{2,30},{3,31},{4,24},{5,25},{6,26},{7,27},{8,20},{9,... | collective-permute-start | bytes 196616 | tf_op jit(solution)/shard_map/ppermute | solution.py:23
  (39 other events, 592.5 us)

commit v3 on v2

--- a/solution.py
+++ b/solution.py
@@ -60,16 +60,25 @@
     return jnp.dot(left, right, preferred_element_type=jnp.float32)
 
 
-def call(body, ids, operands, outputs, limit, **more):
+def own_place():
+    t = lax.axis_index("tp")
+    return lax.axis_index("ep"), t & (CORES - 1), t // CORES
+
+
+def placed(body):
+    return lambda *refs: body(own_place(), *refs)
+
+
+def call(body, operands, outputs, limit, **more):
     vmem = pl.BlockSpec(memory_space=pltpu.VMEM)
     return pl.pallas_call(
-        body,
-        in_specs=[pl.BlockSpec(memory_space=pltpu.SMEM)] + [vmem] * len(operands),
+        placed(body),
+        in_specs=[vmem] * len(operands),
         out_specs=[vmem] * len(outputs),
         out_shape=[jax.ShapeDtypeStruct(shape, dtype) for shape, dtype in outputs],
         compiler_params=pltpu.CompilerParams(vmem_limit_bytes=limit << 20),
         **more,
-    )(ids, *operands)
+    )(*operands)
 
 
 def core_column(ids, place, other, quarter):
@@ -113,7 +122,7 @@
         def _():
             for k in range(half_ep):
                 at = slice(k * rows, (k + 1) * rows)
-                own, got = (even, odd) if core == 0 else (odd, even)
+                own, got = (even, odd) if core == k.bit_count() & 1 else (odd, even)
                 own[at, :] = (mine[k][...].astype(jnp.float32) * own_gain).astype(jnp.bfloat16)
                 got[at, :] = (theirs[at, :].astype(jnp.float32) * own_gain).astype(jnp.bfloat16)
 
@@ -162,11 +171,12 @@
         proj_y = sum(part[:rows, inner].astype(jnp.float32) for part in parts) * row_scale
         gated.append((state * jax.nn.gelu(proj_y, approximate=True)).astype(jnp.bfloat16))
     gated = jnp.concatenate(gated, axis=1)
+    gated = jnp.concatenate([gated] * (2 if rows < 128 else 1), axis=0)
     for other, target in ((1, send), (0, keep)):
         for place in range(n_tp // CORES):
             columns = pl.ds(core_column(ids, place, other, quarter), quarter)
             at = slice(place * quarter, (place + 1) * quarter)
-            target[:, at] = dot32(gated, out_weight[:, columns]).astype(jnp.bfloat16)
+            target[:, at] = dot32(gated, out_weight[:, columns])[:rows].astype(jnp.bfloat16)
 
 
 def dispatch_body(n_y, far, ids, tokens, first, second, gain, chosen, mixed, *refs):
@@ -252,8 +262,7 @@
     n_ep, n_tp = lax.axis_size("ep"), lax.axis_size("tp")
     n_y = n_tp // CORES
     e, t = lax.axis_index("ep").astype(jnp.uint32), lax.axis_index("tp").astype(jnp.uint32)
-    core, y = t & (CORES - 1), t // CORES
-    ids = jnp.stack([e, core, y]).astype(jnp.int32)
+    core = t & (CORES - 1)
     rows, width = tokens.shape
     block, quarter, half = width // n_ep, width // n_tp, width // CORES
     channels = state_in.shape[1]
@@ -266,17 +275,18 @@
     half_ep = n_ep // CORES
     mine = [None] * half_ep
     for k in reversed(range(half_ep)):
-        piece = lax.dynamic_slice_in_dim(tokens, (e ^ (CORES * k + core)) * block, block, 1)
-        mine[k] = send_to(piece, lambda a, b: (a ^ (CORES * k + b % CORES), b))
+        odd_one = k.bit_count() & 1
+        piece = lax.dynamic_slice_in_dim(tokens, (e ^ (CORES * k + (core ^ odd_one))) * block, block, 1)
+        mine[k] = send_to(piece, lambda a, b: (a ^ (CORES * k + (b % CORES ^ odd_one)), b))
     theirs = across_cores(jnp.concatenate(mine, axis=0))
     chosen, combine, scale, decay = call(
-        functools.partial(prepare_body, capacity), ids,
+        functools.partial(prepare_body, capacity),
         [routes.T, route_prob.T, tokens, rate_param[None, :]],
         [((slots, rows), bf16), ((2 * rows, slots), bf16), ((rows, 1), f32), ((1, channels), f32)],
         8,
     )
     even, odd = call(
-        functools.partial(unpack_body, half_ep), ids,
+        functools.partial(unpack_body, half_ep),
         [*mine, theirs, mix_gain.reshape(n_ep, block).astype(f32)],
         [((half_ep * rows, block), bf16)] * 2, 8,
     )
@@ -289,7 +299,7 @@
     addends_x = halving_sum(blocks, rnn_weight, bits)
     addends_y = halving_sum(blocks, gate_weight, swapped)
     state_out, window, keep, send = call(
-        functools.partial(mixer_body, len(addends_x), n_tp), ids,
+        functools.partial(mixer_body, len(addends_x), n_tp),
         [
             *addends_x, *addends_y, scale, state_in, jnp.transpose(conv_in, (1, 0, 2)), conv_weight, decay,
             rate_weight, input_weight, out_weight,
@@ -311,15 +321,15 @@
     late = list(range(n_ep // 2, 3 * n_ep // 4))
     second_gain = moe_gain[None, :].astype(f32)
     mixed, *sends = pl.pallas_call(
-        functools.partial(dispatch_body, n_y, len(near)),
-        in_specs=[pl.BlockSpec(memory_space=pltpu.SMEM)] + [pl.BlockSpec(memory_space=pltpu.VMEM)] * 5,
+        placed(functools.partial(dispatch_body, n_y, len(near))),
+        in_specs=[pl.BlockSpec(memory_space=pltpu.VMEM)] * 5,
         out_specs=[pl.BlockSpec(memory_space=pltpu.VMEM)] * (1 + n_ep),
         out_shape=[jax.ShapeDtypeStruct((rows, half), f32)]
         + [jax.ShapeDtypeStruct((capacity, half if d in near else quarter), bf16) for d in range(n_ep)],
         scratch_shapes=[pltpu.VMEM((rows, half), bf16)],
         compiler_params=pltpu.CompilerParams(vmem_limit_bytes=8 << 20),
         name="dispatch",
-    )(ids, tokens, first, second, second_gain, chosen)
+    )(tokens, first, second, second_gain, chosen)
 
     landed = {0: sends[0]}
     for group in (early, near[1:], late):
@@ -333,7 +343,7 @@
         others = [across_cores(piece) for piece in pieces]
         count = len(group) * capacity
         keep, send = call(
-            functools.partial(expert_body, n_tp, len(pieces), name != "near"), ids,
+            functools.partial(expert_body, n_tp, len(pieces), name != "near"),
             [*pieces, *others, second_gain, expert_gate, expert_up, expert_down], [((count, half), bf16)] * 2,
             20,
             cost_estimate=pl.CostEstimate(
@@ -350,7 +360,7 @@
             piece = total[place * capacity:(place + 1) * capacity]
             back[d] = across_ep(piece, d) if d else piece
     (layer_out,) = call(
-        finish_body, ids, [jnp.concatenate([back[d] for d in range(n_ep)], axis=0), mixed, combine],
+        finish_body, [jnp.concatenate([back[d] for d in range(n_ep)], axis=0), mixed, combine],
         [((rows, quarter), bf16)], 8,
     )
     return (layer_out, state_out, conv_out)

time: 131 us -> 127 us (0.969)
  Pallas kernels: 15 us -> 10.5 us
  starting transfers between devices: 49.9 us -> 53.2 us
  waiting for transfers between devices: 58.5 us -> 55.8 us
    pallas_call x8, Pallas kernels: 15 us -> 10.5 us  [the longest x7 9.99 us: call(): pl.pallas_call(placed(body), in_specs=[vmem] * len(operands), out_specs=[...]
    ppermute x46, starting transfers between devices: 49.9 us -> 53.2 us  [send_to(): return lax.ppermute(value, AXES, pairs)]
    ppermute x46, waiting for transfers between devices: 58.5 us -> 55.8 us  [send_to(): return lax.ppermute(value, AXES, pairs)]
  transfers between devices with their start and end apart: 46 -> 46, of which waited for: 25 -> 25; matrix products, arithmetic and copies ran while one was open for 2% -> 2% of each run, Pallas kernels for 6% -> 5%
where the time goes in v3:
time: 127 us
  waiting for transfers between devices  55.8 us (44%)
  starting transfers between devices  53.2 us (42%)
  Pallas kernels  10.5 us (8%)
  matrix products  3.55 us (3%)
  local copies, waits for them, and re-layouts  2.09 us (2%)
    ppermute x46, waiting for transfers between devices, send_to(): return lax.ppermute(value, AXES, pairs)  55.8 us
    ppermute x46, starting transfers between devices, send_to(): return lax.ppermute(value, AXES, pairs)  53.2 us
    pallas_call x7, Pallas kernels, call(): pl.pallas_call(placed(body), in_specs=[vmem] * len(operands), out_specs=[...  9.99 us
    dot_general x8, matrix products, dot32(): return jnp.dot(left, right, preferred_element_type=jnp.float32)  3.55 us
  transfers between devices with their start and end apart: 46, of which 25 were waited for; matrix products, arithmetic and copies ran while one was open for 2% of the time, Pallas kernels for 5%

profile of v3, /device:TPU:0, one launch (start us, length us, event | category | flops | bytes accessed | tf_op | source)
XLA Modules:
  0.0 127.1 jit_solution(539336796386912113)
XLA Ops:
  2.4 4.0 %collective-permute-start.1 = (bf16[64,512]{1,0:T(8,128)(2,1)S(1)}, bf16[64,512]{1,0:T(8,128)(2,1)S(1)}, u32[]{:S(2)}, u32[]{:S(2)}) collective-permute-start(bf16[64,512]{1,0:T(8,128)(2,1)S(1)} %get-tuple-element.55), channel_id=1, source_target_pairs={{0,12},{1,9},{2,14},{3,11},{4,8},{5,13},{6,10},{7,15},{8,4},{9,1},... | collective-permute-start | bytes 196616 | tf_op jit(solution)/shard_map/ppermute | solution.py:23
  6.4 2.6 %collective-permute-start.2 = (bf16[64,512]{1,0:T(8,128)(2,1)S(1)}, bf16[64,512]{1,0:T(8,128)(2,1)S(1)}, u32[]{:S(2)}, u32[]{:S(2)}) collective-permute-start(bf16[64,512]{1,0:T(8,128)(2,1)S(1)} %get-tuple-element.54), channel_id=1, source_target_pairs={{0,20},{1,17},{2,22},{3,19},{4,16},{5,21},{6,18},{7,23},{8,28},{9,... | collective-permute-start | bytes 196616 | tf_op jit(solution)/shard_map/ppermute | solution.py:23
  9.0 5.4 %collective-permute-done.2.refs_2_ = bf16[64,512]{1,0:T(8,128)(2,1)S(1)} collective-permute-done((bf16[64,512]{1,0:T(8,128)(2,1)S(1)}, bf16[64,512]{1,0:T(8,128)(2,1)S(1)}, u32[]{:S(2)}, u32[]{:S(2)}) %collective-permute-start.2) | collective-permute-done | bytes 65568 | tf_op jit(solution)/shard_map/ppermute | solution.py:23
  25.7 4.4 %collective-permute-done.14.refs_13_ = bf16[256,512]{1,0:T(8,128)(2,1)S(1)} collective-permute-done((bf16[256,512]{1,0:T(8,128)(2,1)S(1)}, bf16[256,512]{1,0:T(8,128)(2,1)S(1)}, u32[]{:S(2)}, u32[]{:S(2)}) %collective-permute-start.14) | collective-permute-done | bytes 262176 | tf_op jit(solution)/shard_map/ppermute | solution.py:23
  31.4 3.6 %collective-permute-done.11.refs_9_ = bf16[256,512]{1,0:T(8,128)(2,1)S(1)} collective-permute-done((bf16[256,512]{1,0:T(8,128)(2,1)S(1)}, bf16[256,512]{1,0:T(8,128)(2,1)S(1)}, u32[]{:S(2)}, u32[]{:S(2)}) %collective-permute-start.11) | collective-permute-done | bytes 262176 | tf_op jit(solution)/shard_map/ppermute | solution.py:23
  41.3 2.1 %collective-permute-start.16 = (bf16[64,512]{1,0:T(8,128)(2,1)S(1)}, bf16[64,512]{1,0:T(8,128)(2,1)S(1)}, u32[]{:S(2)}, u32[]{:S(2)}) collective-permute-start(bf16[64,512]{1,0:T(8,128)(2,1)S(1)} %add_convert_fusion.11), channel_id=1, source_target_pairs={{0,16},{1,17},{2,18},{3,19},{4,20},{5,21},{6,22},{7,23},{8,24},{9,... | collective-permute-start | bytes 196616 | tf_op jit(solution)/shard_map/ppermute | solution.py:23
  48.2 3.0 %collective-permute-done.16.refs_15_ = bf16[64,512]{1,0:T(8,128)(2,1)S(1)} collective-permute-done((bf16[64,512]{1,0:T(8,128)(2,1)S(1)}, bf16[64,512]{1,0:T(8,128)(2,1)S(1)}, u32[]{:S(2)}, u32[]{:S(2)}) %collective-permute-start.16) | collective-permute-done | bytes 65568 | tf_op jit(solution)/shard_map/ppermute | solution.py:23
  51.2 2.1 %collective-permute-done.13.refs_11_ = bf16[64,512]{1,0:T(8,128)(2,1)S(1)} collective-permute-done((bf16[64,512]{1,0:T(8,128)(2,1)S(1)}, bf16[64,512]{1,0:T(8,128)(2,1)S(1)}, u32[]{:S(2)}, u32[]{:S(2)}) %collective-permute-start.13) | collective-permute-done | bytes 65568 | tf_op jit(solution)/shard_map/ppermute | solution.py:23
  55.4 2.6 %shard_map.186 = (f32[64,1024]{1,0:T(8,128)}, bf16[3,64,1024]{2,1,0:T(8,128)(2,1)}, bf16[64,2048]{1,0:T(8,128)(2,1)S(1)}, bf16[64,2048]{1,0:T(8,128)(2,1)S(1)}) custom-call(bf16[256,512]{1,0:T(8,128)(2,1)S(1)} %convolution_convert_fusion.7.refs_0_, bf16[256,512]{1,0:T(8,128)(2,1)S(1)} %collective-permute-done.5.refs_1_, ...), custom_call_target="tpu_custom_call" | custom-call | tf_op jit(solution)/shard_map/pallas_call | solution.py:74
  61.2 6.8 %collective-permute-done.18.refs_2_ = bf16[64,2048]{1,0:T(8,128)(2,1)S(1)} collective-permute-done((bf16[64,2048]{1,0:T(8,128)(2,1)S(1)}, bf16[64,2048]{1,0:T(8,128)(2,1)S(1)}, u32[]{:S(2)}, u32[]{:S(2)}) %collective-permute-start.18) | collective-permute-done | bytes 262176 | tf_op jit(solution)/shard_map/ppermute | solution.py:23
  68.6 1.9 %collective-permute-start.37 = (bf16[32,1024]{1,0:T(8,128)(2,1)S(1)}, bf16[32,1024]{1,0:T(8,128)(2,1)S(1)}, u32[]{:S(2)}, u32[]{:S(2)}) collective-permute-start(bf16[32,1024]{1,0:T(8,128)(2,1)S(1)} %get-tuple-element.45), channel_id=1, source_target_pairs={{0,24},{1,25},{2,26},{3,27},{4,28},{5,29},{6,30},{7,31},{8,16},{9,... | collective-permute-start | bytes 196616 | tf_op jit(solution)/shard_map/ppermute | solution.py:23
  70.5 2.2 %collective-permute-start.38 = (bf16[32,1024]{1,0:T(8,128)(2,1)S(1)}, bf16[32,1024]{1,0:T(8,128)(2,1)S(1)}, u32[]{:S(2)}, u32[]{:S(2)}) collective-permute-start(bf16[32,1024]{1,0:T(8,128)(2,1)S(1)} %get-tuple-element.46), channel_id=1, source_target_pairs={{0,28},{1,29},{2,30},{3,31},{4,24},{5,25},{6,26},{7,27},{8,20},{9,... | collective-permute-start | bytes 196616 | tf_op jit(solution)/shard_map/ppermute | solution.py:23
  72.7 3.6 %collective-permute-start.29 = (bf16[32,1024]{1,0:T(8,128)(2,1)S(1)}, bf16[32,1024]{1,0:T(8,128)(2,1)S(1)}, u32[]{:S(2)}, u32[]{:S(2)}) collective-permute-start(bf16[32,1024]{1,0:T(8,128)(2,1)S(1)} %get-tuple-element.42), channel_id=1, source_target_pairs={{0,20},{1,21},{2,22},{3,23},{4,16},{5,17},{6,18},{7,19},{8,28},{9,... | collective-permute-start | bytes 196616 | tf_op jit(solution)/shard_map/ppermute | solution.py:23
  77.5 2.4 %collective-permute-start.21 = (bf16[32,2048]{1,0:T(8,128)(2,1)S(1)}, bf16[32,2048]{1,0:T(8,128)(2,1)S(1)}, u32[]{:S(2)}, u32[]{:S(2)}) collective-permute-start(bf16[32,2048]{1,0:T(8,128)(2,1)S(1)} %get-tuple-element.38), channel_id=1, source_target_pairs={{0,12},{1,13},{2,14},{3,15},{4,8},{5,9},{6,10},{7,11},{8,4},{9,5},... | collective-permute-start | bytes 393224 | tf_op jit(solution)/shard_map/ppermute | solution.py:23
  85.1 3.0 %collective-permute-done.30.refs_1_ = bf16[64,1024]{1,0:T(8,128)(2,1)S(1)} collective-permute-done((bf16[64,1024]{1,0:T(8,128)(2,1)S(1)}, bf16[64,1024]{1,0:T(8,128)(2,1)S(1)}, u32[]{:S(2)}, u32[]{:S(2)}) %collective-permute-start.30) | collective-permute-done | bytes 131104 | tf_op jit(solution)/shard_map/ppermute | solution.py:23
  88.2 2.0 %shard_map.189 = (bf16[64,2048]{1,0:T(8,128)(2,1)S(1)}, bf16[64,2048]{1,0:T(8,128)(2,1)S(1)}) custom-call(bf16[64,1024]{1,0:T(8,128)(2,1)S(1)} %constant_dynamic-update-slice_fusion.6.refs_0_, bf16[64,1024]{1,0:T(8,128)(2,1)S(1)} %collective-permute-done.39.refs_1_, bf16[64,1024]{1,0:T(8,128)(2,1)S(1)} %collective-permute-done.40.refs_2_, ...), custom_call_target="tpu_custom_call" | custom-call | flops 805306368 | tf_op jit(solution)/shard_map/pallas_call | solution.py:74
  90.9 2.0 %shard_map.188 = (bf16[64,2048]{1,0:T(8,128)(2,1)S(1)}, bf16[64,2048]{1,0:T(8,128)(2,1)S(1)}) custom-call(bf16[64,1024]{1,0:T(8,128)(2,1)S(1)} %constant_dynamic-update-slice_fusion.4.refs_0_, bf16[64,1024]{1,0:T(8,128)(2,1)S(1)} %collective-permute-done.30.refs_1_, bf16[64,1024]{1,0:T(8,128)(2,1)S(1)} %collective-permute-done.31.refs_2_, ...), custom_call_target="tpu_custom_call" | custom-call | flops 805306368 | tf_op jit(solution)/shard_map/pallas_call | solution.py:74
  95.2 2.0 %shard_map.187 = (bf16[128,2048]{1,0:T(8,128)(2,1)S(1)}, bf16[128,2048]{1,0:T(8,128)(2,1)S(1)}) custom-call(bf16[128,2048]{1,0:T(8,128)(2,1)S(1)} %constant_dynamic-update-slice_fusion.refs_0_, bf16[128,2048]{1,0:T(8,128)(2,1)S(1)} %collective-permute-done.22.refs_1_, f32[1,4096]{1,0:T(1,128)S(1)} %bitcast.11, bf16[1,4096,512]{2,1,0:T(8,128)(2,1)S(1)} %copy-done, ...), custom_call_target="tpu_custom_call" | custom-call | flops 1610612736 | tf_op jit(solution)/shard_map/pallas_call | solution.py:74
  100.9 1.9 %collective-permute-start.44 = (bf16[32,1024]{1,0:T(8,128)(2,1)S(1)}, bf16[32,1024]{1,0:T(8,128)(2,1)S(1)}, u32[]{:S(2)}, u32[]{:S(2)}) collective-permute-start(bf16[32,1024]{1,0:T(8,128)(2,1)S(1)} %get-tuple-element.70), channel_id=1, source_target_pairs={{0,24},{1,25},{2,26},{3,27},{4,28},{5,29},{6,30},{7,31},{8,16},{9,... | collective-permute-start | bytes 196616 | tf_op jit(solution)/shard_map/ppermute | solution.py:23
  103.9 5.1 %collective-permute-done.24 = bf16[128,1024]{1,0:T(8,128)(2,1)S(1)} collective-permute-done((bf16[128,1024]{1,0:T(8,128)(2,1)S(1)}, bf16[128,1024]{1,0:T(8,128)(2,1)S(1)}, u32[]{:S(2)}, u32[]{:S(2)}) %collective-permute-start.24) | collective-permute-done | bytes 262176 | tf_op jit(solution)/shard_map/ppermute | solution.py:23
  110.6 3.0 %collective-permute-start.36 = (bf16[32,1024]{1,0:T(8,128)(2,1)S(1)}, bf16[32,1024]{1,0:T(8,128)(2,1)S(1)}, u32[]{:S(2)}, u32[]{:S(2)}) collective-permute-start(bf16[32,1024]{1,0:T(8,128)(2,1)S(1)} %get-tuple-element.71), channel_id=1, source_target_pairs={{0,20},{1,21},{2,22},{3,23},{4,16},{5,17},{6,18},{7,19},{8,28},{9,... | collective-permute-start | bytes 196616 | tf_op jit(solution)/shard_map/ppermute | solution.py:23
  113.6 2.4 %collective-permute-start.45 = (bf16[32,1024]{1,0:T(8,128)(2,1)S(1)}, bf16[32,1024]{1,0:T(8,128)(2,1)S(1)}, u32[]{:S(2)}, u32[]{:S(2)}) collective-permute-start(bf16[32,1024]{1,0:T(8,128)(2,1)S(1)} %get-tuple-element.69), channel_id=1, source_target_pairs={{0,28},{1,29},{2,30},{3,31},{4,24},{5,25},{6,26},{7,27},{8,20},{9,... | collective-permute-start | bytes 196616 | tf_op jit(solution)/shard_map/ppermute | solution.py:23
  116.0 4.9 %collective-permute-done.26 = bf16[32,1024]{1,0:T(8,128)(2,1)S(1)} collective-permute-done((bf16[32,1024]{1,0:T(8,128)(2,1)S(1)}, bf16[32,1024]{1,0:T(8,128)(2,1)S(1)}, u32[]{:S(2)}, u32[]{:S(2)}) %collective-permute-start.26) | collective-permute-done | bytes 65568 | tf_op jit(solution)/shard_map/ppermute | solution.py:23
  121.3 4.8 %collective-permute-done.27 = bf16[32,1024]{1,0:T(8,128)(2,1)S(1)} collective-permute-done((bf16[32,1024]{1,0:T(8,128)(2,1)S(1)}, bf16[32,1024]{1,0:T(8,128)(2,1)S(1)}, u32[]{:S(2)}, u32[]{:S(2)}) %collective-permute-start.27) | collective-permute-done | bytes 65568 | tf_op jit(solution)/shard_map/ppermute | solution.py:23
  (160 shorter events, 47.7 us)
Async XLA Ops:
  1.7 7.3 %collective-permute-start = (bf16[64,512]{1,0:T(8,128)(2,1)S(1)}, bf16[64,512]{1,0:T(8,128)(2,1)S(1)}, u32[]{:S(2)}, u32[]{:S(2)}) collective-permute-start(bf16[64,512]{1,0:T(8,128)(2,1)S(1)} %get-tuple-element.56), channel_id=1, source_target_pairs={{0,0},{1,5},{2,2},{3,7},{4,4},{5,1},{6,6},{7,3},{8,8},{9,13},{10,1... | collective-permute-start | bytes 196616 | tf_op jit(solution)/shard_map/ppermute | solution.py:23
  6.4 7.9 %collective-permute-start.2 = (bf16[64,512]{1,0:T(8,128)(2,1)S(1)}, bf16[64,512]{1,0:T(8,128)(2,1)S(1)}, u32[]{:S(2)}, u32[]{:S(2)}) collective-permute-start(bf16[64,512]{1,0:T(8,128)(2,1)S(1)} %get-tuple-element.54), channel_id=1, source_target_pairs={{0,20},{1,17},{2,22},{3,19},{4,16},{5,21},{6,18},{7,23},{8,28},{9,... | collective-permute-start | bytes 196616 | tf_op jit(solution)/shard_map/ppermute | solution.py:23
  20.8 9.2 %collective-permute-start.14 = (bf16[256,512]{1,0:T(8,128)(2,1)S(1)}, bf16[256,512]{1,0:T(8,128)(2,1)S(1)}, u32[]{:S(2)}, u32[]{:S(2)}) collective-permute-start(bf16[256,512]{1,0:T(8,128)(2,1)S(1)} %convolution_convert_fusion), channel_id=1, source_target_pairs={{0,8},{1,9},{2,10},{3,11},{4,12},{5,13},{6,14},{7,15},{8,0},{9,1},... | collective-permute-start | bytes 786440 | tf_op jit(solution)/shard_map/ppermute | solution.py:23
  22.2 12.9 %collective-permute-start.11 = (bf16[256,512]{1,0:T(8,128)(2,1)S(1)}, bf16[256,512]{1,0:T(8,128)(2,1)S(1)}, u32[]{:S(2)}, u32[]{:S(2)}) collective-permute-start(bf16[256,512]{1,0:T(8,128)(2,1)S(1)} %convolution_convert_fusion.2), channel_id=1, source_target_pairs={{0,8},{1,9},{2,10},{3,11},{4,12},{5,13},{6,14},{7,15},{8,0},{9,1},... | collective-permute-start | bytes 786440 | tf_op jit(solution)/shard_map/ppermute | solution.py:23
  23.6 12.6 %collective-permute-start.8 = (bf16[256,512]{1,0:T(8,128)(2,1)S(1)}, bf16[256,512]{1,0:T(8,128)(2,1)S(1)}, u32[]{:S(2)}, u32[]{:S(2)}) collective-permute-start(bf16[256,512]{1,0:T(8,128)(2,1)S(1)} %convolution_convert_fusion.4), channel_id=1, source_target_pairs={{0,4},{1,5},{2,6},{3,7},{4,0},{5,1},{6,2},{7,3},{8,12},{9,13},{10,... | collective-permute-start | bytes 786440 | tf_op jit(solution)/shard_map/ppermute | solution.py:23
  24.9 13.5 %collective-permute-start.5 = (bf16[256,512]{1,0:T(8,128)(2,1)S(1)}, bf16[256,512]{1,0:T(8,128)(2,1)S(1)}, u32[]{:S(2)}, u32[]{:S(2)}) collective-permute-start(bf16[256,512]{1,0:T(8,128)(2,1)S(1)} %convolution_convert_fusion.6), channel_id=1, source_target_pairs={{0,4},{1,5},{2,6},{3,7},{4,0},{5,1},{6,2},{7,3},{8,12},{9,13},{10,... | collective-permute-start | bytes 786440 | tf_op jit(solution)/shard_map/ppermute | solution.py:23
  30.1 11.2 %collective-permute-start.15 = (bf16[128,512]{1,0:T(8,128)(2,1)S(1)}, bf16[128,512]{1,0:T(8,128)(2,1)S(1)}, u32[]{:S(2)}, u32[]{:S(2)}) collective-permute-start(bf16[128,512]{1,0:T(8,128)(2,1)S(1)} %add_convert_fusion.7), channel_id=1, source_target_pairs={{0,4},{1,5},{2,6},{3,7},{4,0},{5,1},{6,2},{7,3},{8,12},{9,13},{10,... | collective-permute-start | bytes 393224 | tf_op jit(solution)/shard_map/ppermute | solution.py:23
  35.1 8.3 %collective-permute-start.12 = (bf16[128,512]{1,0:T(8,128)(2,1)S(1)}, bf16[128,512]{1,0:T(8,128)(2,1)S(1)}, u32[]{:S(2)}, u32[]{:S(2)}) collective-permute-start(bf16[128,512]{1,0:T(8,128)(2,1)S(1)} %add_convert_fusion.8), channel_id=1, source_target_pairs={{0,4},{1,5},{2,6},{3,7},{4,0},{5,1},{6,2},{7,3},{8,12},{9,13},{10,... | collective-permute-start | bytes 393224 | tf_op jit(solution)/shard_map/ppermute | solution.py:23
  36.3 8.6 %collective-permute-start.9 = (bf16[128,512]{1,0:T(8,128)(2,1)S(1)}, bf16[128,512]{1,0:T(8,128)(2,1)S(1)}, u32[]{:S(2)}, u32[]{:S(2)}) collective-permute-start(bf16[128,512]{1,0:T(8,128)(2,1)S(1)} %add_convert_fusion.9), channel_id=1, source_target_pairs={{0,8},{1,9},{2,10},{3,11},{4,12},{5,13},{6,14},{7,15},{8,0},{9,1},... | collective-permute-start | bytes 393224 | tf_op jit(solution)/shard_map/ppermute | solution.py:23
  38.5 8.1 %collective-permute-start.6 = (bf16[128,512]{1,0:T(8,128)(2,1)S(1)}, bf16[128,512]{1,0:T(8,128)(2,1)S(1)}, u32[]{:S(2)}, u32[]{:S(2)}) collective-permute-start(bf16[128,512]{1,0:T(8,128)(2,1)S(1)} %add_convert_fusion.10), channel_id=1, source_target_pairs={{0,8},{1,9},{2,10},{3,11},{4,12},{5,13},{6,14},{7,15},{8,0},{9,1},... | collective-permute-start | bytes 393224 | tf_op jit(solution)/shard_map/ppermute | solution.py:23
  41.3 9.9 %collective-permute-start.16 = (bf16[64,512]{1,0:T(8,128)(2,1)S(1)}, bf16[64,512]{1,0:T(8,128)(2,1)S(1)}, u32[]{:S(2)}, u32[]{:S(2)}) collective-permute-start(bf16[64,512]{1,0:T(8,128)(2,1)S(1)} %add_convert_fusion.11), channel_id=1, source_target_pairs={{0,16},{1,17},{2,18},{3,19},{4,20},{5,21},{6,22},{7,23},{8,24},{9,... | collective-permute-start | bytes 196616 | tf_op jit(solution)/shard_map/ppermute | solution.py:23
  43.4 9.9 %collective-permute-start.13 = (bf16[64,512]{1,0:T(8,128)(2,1)S(1)}, bf16[64,512]{1,0:T(8,128)(2,1)S(1)}, u32[]{:S(2)}, u32[]{:S(2)}) collective-permute-start(bf16[64,512]{1,0:T(8,128)(2,1)S(1)} %add_convert_fusion.12), channel_id=1, source_target_pairs={{0,16},{1,17},{2,18},{3,19},{4,20},{5,21},{6,22},{7,23},{8,24},{9,... | collective-permute-start | bytes 196616 | tf_op jit(solution)/shard_map/ppermute | solution.py:23
  44.9 9.7 %collective-permute-start.10 = (bf16[64,512]{1,0:T(8,128)(2,1)S(1)}, bf16[64,512]{1,0:T(8,128)(2,1)S(1)}, u32[]{:S(2)}, u32[]{:S(2)}) collective-permute-start(bf16[64,512]{1,0:T(8,128)(2,1)S(1)} %add_convert_fusion.13), channel_id=1, source_target_pairs={{0,16},{1,17},{2,18},{3,19},{4,20},{5,21},{6,22},{7,23},{8,24},{9,... | collective-permute-start | bytes 196616 | tf_op jit(solution)/shard_map/ppermute | solution.py:23
  46.6 8.7 %collective-permute-start.7 = (bf16[64,512]{1,0:T(8,128)(2,1)S(1)}, bf16[64,512]{1,0:T(8,128)(2,1)S(1)}, u32[]{:S(2)}, u32[]{:S(2)}) collective-permute-start(bf16[64,512]{1,0:T(8,128)(2,1)S(1)} %add_convert_fusion.14), channel_id=1, source_target_pairs={{0,16},{1,17},{2,18},{3,19},{4,20},{5,21},{6,22},{7,23},{8,24},{9,... | collective-permute-start | bytes 196616 | tf_op jit(solution)/shard_map/ppermute | solution.py:23
  59.6 8.4 %collective-permute-start.18 = (bf16[64,2048]{1,0:T(8,128)(2,1)S(1)}, bf16[64,2048]{1,0:T(8,128)(2,1)S(1)}, u32[]{:S(2)}, u32[]{:S(2)}) collective-permute-start(bf16[64,2048]{1,0:T(8,128)(2,1)S(1)} %add_convert_fusion.4.refs_1_), channel_id=1, source_target_pairs={{0,2},{1,3},{2,0},{3,1},{4,6},{5,7},{6,4},{7,5},{8,10},{9,11},{10,... | collective-permute-start | bytes 786440 | tf_op jit(solution)/shard_map/ppermute | solution.py:23
  68.6 8.6 %collective-permute-start.37 = (bf16[32,1024]{1,0:T(8,128)(2,1)S(1)}, bf16[32,1024]{1,0:T(8,128)(2,1)S(1)}, u32[]{:S(2)}, u32[]{:S(2)}) collective-permute-start(bf16[32,1024]{1,0:T(8,128)(2,1)S(1)} %get-tuple-element.45), channel_id=1, source_target_pairs={{0,24},{1,25},{2,26},{3,27},{4,28},{5,29},{6,30},{7,31},{8,16},{9,... | collective-permute-start | bytes 196616 | tf_op jit(solution)/shard_map/ppermute | solution.py:23
  72.7 9.4 %collective-permute-start.29 = (bf16[32,1024]{1,0:T(8,128)(2,1)S(1)}, bf16[32,1024]{1,0:T(8,128)(2,1)S(1)}, u32[]{:S(2)}, u32[]{:S(2)}) collective-permute-start(bf16[32,1024]{1,0:T(8,128)(2,1)S(1)} %get-tuple-element.42), channel_id=1, source_target_pairs={{0,20},{1,21},{2,22},{3,23},{4,16},{5,17},{6,18},{7,19},{8,28},{9,... | collective-permute-start | bytes 196616 | tf_op jit(solution)/shard_map/ppermute | solution.py:23
  77.2 7.4 %collective-permute-start.20 = (bf16[32,2048]{1,0:T(8,128)(2,1)S(1)}, bf16[32,2048]{1,0:T(8,128)(2,1)S(1)}, u32[]{:S(2)}, u32[]{:S(2)}) collective-permute-start(bf16[32,2048]{1,0:T(8,128)(2,1)S(1)} %get-tuple-element.37), channel_id=1, source_target_pairs={{0,8},{1,9},{2,10},{3,11},{4,12},{5,13},{6,14},{7,15},{8,0},{9,1},... | collective-permute-start | bytes 393224 | tf_op jit(solution)/shard_map/ppermute | solution.py:23
  77.5 13.3 %collective-permute-start.21 = (bf16[32,2048]{1,0:T(8,128)(2,1)S(1)}, bf16[32,2048]{1,0:T(8,128)(2,1)S(1)}, u32[]{:S(2)}, u32[]{:S(2)}) collective-permute-start(bf16[32,2048]{1,0:T(8,128)(2,1)S(1)} %get-tuple-element.38), channel_id=1, source_target_pairs={{0,12},{1,13},{2,14},{3,15},{4,8},{5,9},{6,10},{7,11},{8,4},{9,5},... | collective-permute-start | bytes 393224 | tf_op jit(solution)/shard_map/ppermute | solution.py:23
  99.3 9.6 %collective-permute-start.24 = (bf16[128,1024]{1,0:T(8,128)(2,1)S(1)}, bf16[128,1024]{1,0:T(8,128)(2,1)S(1)}, u32[]{:S(2)}, u32[]{:S(2)}) collective-permute-start(bf16[128,1024]{1,0:T(8,128)(2,1)S(1)} %slice.205), channel_id=1, source_target_pairs={{0,2},{1,3},{2,0},{3,1},{4,6},{5,7},{6,4},{7,5},{8,10},{9,11},{10,... | collective-permute-start | bytes 786440 | tf_op jit(solution)/shard_map/ppermute | solution.py:23
  100.9 25.3 %collective-permute-start.44 = (bf16[32,1024]{1,0:T(8,128)(2,1)S(1)}, bf16[32,1024]{1,0:T(8,128)(2,1)S(1)}, u32[]{:S(2)}, u32[]{:S(2)}) collective-permute-start(bf16[32,1024]{1,0:T(8,128)(2,1)S(1)} %get-tuple-element.70), channel_id=1, source_target_pairs={{0,24},{1,25},{2,26},{3,27},{4,28},{5,29},{6,30},{7,31},{8,16},{9,... | collective-permute-start | bytes 196616 | tf_op jit(solution)/shard_map/ppermute | solution.py:23
  110.2 15.9 %collective-permute-start.35 = (bf16[32,1024]{1,0:T(8,128)(2,1)S(1)}, bf16[32,1024]{1,0:T(8,128)(2,1)S(1)}, u32[]{:S(2)}, u32[]{:S(2)}) collective-permute-start(bf16[32,1024]{1,0:T(8,128)(2,1)S(1)} %get-tuple-element.72), channel_id=1, source_target_pairs={{0,16},{1,17},{2,18},{3,19},{4,20},{5,21},{6,22},{7,23},{8,24},{9,... | collective-permute-start | bytes 196616 | tf_op jit(solution)/shard_map/ppermute | solution.py:23
  110.6 15.5 %collective-permute-start.36 = (bf16[32,1024]{1,0:T(8,128)(2,1)S(1)}, bf16[32,1024]{1,0:T(8,128)(2,1)S(1)}, u32[]{:S(2)}, u32[]{:S(2)}) collective-permute-start(bf16[32,1024]{1,0:T(8,128)(2,1)S(1)} %get-tuple-element.71), channel_id=1, source_target_pairs={{0,20},{1,21},{2,22},{3,23},{4,16},{5,17},{6,18},{7,19},{8,28},{9,... | collective-permute-start | bytes 196616 | tf_op jit(solution)/shard_map/ppermute | solution.py:23
  113.6 12.6 %collective-permute-start.45 = (bf16[32,1024]{1,0:T(8,128)(2,1)S(1)}, bf16[32,1024]{1,0:T(8,128)(2,1)S(1)}, u32[]{:S(2)}, u32[]{:S(2)}) collective-permute-start(bf16[32,1024]{1,0:T(8,128)(2,1)S(1)} %get-tuple-element.69), channel_id=1, source_target_pairs={{0,28},{1,29},{2,30},{3,31},{4,24},{5,25},{6,26},{7,27},{8,20},{9,... | collective-permute-start | bytes 196616 | tf_op jit(solution)/shard_map/ppermute | solution.py:23
  (39 other events, 589.5 us)

commit v4 on v3

--- a/solution.py
+++ b/solution.py
@@ -187,7 +187,9 @@
         columns = pl.ds(core_column(ids, place, 0, quarter), quarter)
         base = tokens[:, columns].astype(jnp.float32)
         part = base + (first[:, at].astype(jnp.float32) + second[:, at].astype(jnp.float32))
-        mixed[:, at] = part
+        @pl.when(ids[2] == place)
+        def _(part=part):
+            mixed[...] = part
         gained[:, at] = (part * gain[:, columns]).astype(jnp.bfloat16)
     capacity = sends[0].shape[0]
     split = far * capacity
@@ -234,8 +236,8 @@
 
 
 def finish_body(ids, returned, mixed, combine, layer):
-    rows, quarter = layer.shape
-    base = mixed[:, pl.ds(pl.multiple_of(ids[2] * quarter, 128), quarter)]
+    rows, _ = layer.shape
+    base = mixed[...]
     both = dot32(combine[...], returned[...])
     layer[...] = (base + (both[:rows] + both[rows:])).astype(jnp.bfloat16)
 
@@ -324,7 +326,7 @@
         placed(functools.partial(dispatch_body, n_y, len(near))),
         in_specs=[pl.BlockSpec(memory_space=pltpu.VMEM)] * 5,
         out_specs=[pl.BlockSpec(memory_space=pltpu.VMEM)] * (1 + n_ep),
-        out_shape=[jax.ShapeDtypeStruct((rows, half), f32)]
+        out_shape=[jax.ShapeDtypeStruct((rows, quarter), f32)]
         + [jax.ShapeDtypeStruct((capacity, half if d in near else quarter), bf16) for d in range(n_ep)],
         scratch_shapes=[pltpu.VMEM((rows, half), bf16)],
         compiler_params=pltpu.CompilerParams(vmem_limit_bytes=8 << 20),

time: 127 us -> 127 us (level)
  no operation moved by 1% of the time
where the time goes in v4:
time: 127 us
  waiting for transfers between devices  55.7 us (44%)
  starting transfers between devices  53.2 us (42%)
  Pallas kernels  10.7 us (8%)
  matrix products  3.56 us (3%)
  local copies, waits for them, and re-layouts  2.09 us (2%)
    ppermute x46, waiting for transfers between devices, send_to(): return lax.ppermute(value, AXES, pairs)  55.7 us
    ppermute x46, starting transfers between devices, send_to(): return lax.ppermute(value, AXES, pairs)  53.2 us
    pallas_call x7, Pallas kernels, call(): pl.pallas_call(placed(body), in_specs=[vmem] * len(operands), out_specs=[...  9.98 us
    dot_general x8, matrix products, dot32(): return jnp.dot(left, right, preferred_element_type=jnp.float32)  3.56 us
  transfers between devices with their start and end apart: 46, of which 25 were waited for; matrix products, arithmetic and copies ran while one was open for 2% of the time, Pallas kernels for 5%

profile of v4, /device:TPU:0, one launch (start us, length us, event | category | flops | bytes accessed | tf_op | source)
XLA Modules:
  0.0 127.3 jit_solution(9354662088244724363)
XLA Ops:
  2.4 4.0 %collective-permute-start.1 = (bf16[64,512]{1,0:T(8,128)(2,1)S(1)}, bf16[64,512]{1,0:T(8,128)(2,1)S(1)}, u32[]{:S(2)}, u32[]{:S(2)}) collective-permute-start(bf16[64,512]{1,0:T(8,128)(2,1)S(1)} %get-tuple-element.55), channel_id=1, source_target_pairs={{0,12},{1,9},{2,14},{3,11},{4,8},{5,13},{6,10},{7,15},{8,4},{9,1},... | collective-permute-start | bytes 196616 | tf_op jit(solution)/shard_map/ppermute | solution.py:23
  6.4 2.6 %collective-permute-start.2 = (bf16[64,512]{1,0:T(8,128)(2,1)S(1)}, bf16[64,512]{1,0:T(8,128)(2,1)S(1)}, u32[]{:S(2)}, u32[]{:S(2)}) collective-permute-start(bf16[64,512]{1,0:T(8,128)(2,1)S(1)} %get-tuple-element.54), channel_id=1, source_target_pairs={{0,20},{1,17},{2,22},{3,19},{4,16},{5,21},{6,18},{7,23},{8,28},{9,... | collective-permute-start | bytes 196616 | tf_op jit(solution)/shard_map/ppermute | solution.py:23
  9.0 5.4 %collective-permute-done.2.refs_2_ = bf16[64,512]{1,0:T(8,128)(2,1)S(1)} collective-permute-done((bf16[64,512]{1,0:T(8,128)(2,1)S(1)}, bf16[64,512]{1,0:T(8,128)(2,1)S(1)}, u32[]{:S(2)}, u32[]{:S(2)}) %collective-permute-start.2) | collective-permute-done | bytes 65568 | tf_op jit(solution)/shard_map/ppermute | solution.py:23
  25.7 4.4 %collective-permute-done.14.refs_13_ = bf16[256,512]{1,0:T(8,128)(2,1)S(1)} collective-permute-done((bf16[256,512]{1,0:T(8,128)(2,1)S(1)}, bf16[256,512]{1,0:T(8,128)(2,1)S(1)}, u32[]{:S(2)}, u32[]{:S(2)}) %collective-permute-start.14) | collective-permute-done | bytes 262176 | tf_op jit(solution)/shard_map/ppermute | solution.py:23
  31.5 3.6 %collective-permute-done.11.refs_9_ = bf16[256,512]{1,0:T(8,128)(2,1)S(1)} collective-permute-done((bf16[256,512]{1,0:T(8,128)(2,1)S(1)}, bf16[256,512]{1,0:T(8,128)(2,1)S(1)}, u32[]{:S(2)}, u32[]{:S(2)}) %collective-permute-start.11) | collective-permute-done | bytes 262176 | tf_op jit(solution)/shard_map/ppermute | solution.py:23
  41.3 2.1 %collective-permute-start.16 = (bf16[64,512]{1,0:T(8,128)(2,1)S(1)}, bf16[64,512]{1,0:T(8,128)(2,1)S(1)}, u32[]{:S(2)}, u32[]{:S(2)}) collective-permute-start(bf16[64,512]{1,0:T(8,128)(2,1)S(1)} %add_convert_fusion.11), channel_id=1, source_target_pairs={{0,16},{1,17},{2,18},{3,19},{4,20},{5,21},{6,22},{7,23},{8,24},{9,... | collective-permute-start | bytes 196616 | tf_op jit(solution)/shard_map/ppermute | solution.py:23
  48.2 3.0 %collective-permute-done.16.refs_15_ = bf16[64,512]{1,0:T(8,128)(2,1)S(1)} collective-permute-done((bf16[64,512]{1,0:T(8,128)(2,1)S(1)}, bf16[64,512]{1,0:T(8,128)(2,1)S(1)}, u32[]{:S(2)}, u32[]{:S(2)}) %collective-permute-start.16) | collective-permute-done | bytes 65568 | tf_op jit(solution)/shard_map/ppermute | solution.py:23
  51.2 2.1 %collective-permute-done.13.refs_11_ = bf16[64,512]{1,0:T(8,128)(2,1)S(1)} collective-permute-done((bf16[64,512]{1,0:T(8,128)(2,1)S(1)}, bf16[64,512]{1,0:T(8,128)(2,1)S(1)}, u32[]{:S(2)}, u32[]{:S(2)}) %collective-permute-start.13) | collective-permute-done | bytes 65568 | tf_op jit(solution)/shard_map/ppermute | solution.py:23
  55.4 2.6 %shard_map.186 = (f32[64,1024]{1,0:T(8,128)}, bf16[3,64,1024]{2,1,0:T(8,128)(2,1)}, bf16[64,2048]{1,0:T(8,128)(2,1)S(1)}, bf16[64,2048]{1,0:T(8,128)(2,1)S(1)}) custom-call(bf16[256,512]{1,0:T(8,128)(2,1)S(1)} %convolution_convert_fusion.7.refs_0_, bf16[256,512]{1,0:T(8,128)(2,1)S(1)} %collective-permute-done.5.refs_1_, ...), custom_call_target="tpu_custom_call" | custom-call | tf_op jit(solution)/shard_map/pallas_call | solution.py:74
  61.2 6.8 %collective-permute-done.18.refs_2_ = bf16[64,2048]{1,0:T(8,128)(2,1)S(1)} collective-permute-done((bf16[64,2048]{1,0:T(8,128)(2,1)S(1)}, bf16[64,2048]{1,0:T(8,128)(2,1)S(1)}, u32[]{:S(2)}, u32[]{:S(2)}) %collective-permute-start.18) | collective-permute-done | bytes 262176 | tf_op jit(solution)/shard_map/ppermute | solution.py:23
  68.7 1.9 %collective-permute-start.37 = (bf16[32,1024]{1,0:T(8,128)(2,1)S(1)}, bf16[32,1024]{1,0:T(8,128)(2,1)S(1)}, u32[]{:S(2)}, u32[]{:S(2)}) collective-permute-start(bf16[32,1024]{1,0:T(8,128)(2,1)S(1)} %get-tuple-element.45), channel_id=1, source_target_pairs={{0,24},{1,25},{2,26},{3,27},{4,28},{5,29},{6,30},{7,31},{8,16},{9,... | collective-permute-start | bytes 196616 | tf_op jit(solution)/shard_map/ppermute | solution.py:23
  70.7 2.2 %collective-permute-start.38 = (bf16[32,1024]{1,0:T(8,128)(2,1)S(1)}, bf16[32,1024]{1,0:T(8,128)(2,1)S(1)}, u32[]{:S(2)}, u32[]{:S(2)}) collective-permute-start(bf16[32,1024]{1,0:T(8,128)(2,1)S(1)} %get-tuple-element.46), channel_id=1, source_target_pairs={{0,28},{1,29},{2,30},{3,31},{4,24},{5,25},{6,26},{7,27},{8,20},{9,... | collective-permute-start | bytes 196616 | tf_op jit(solution)/shard_map/ppermute | solution.py:23
  72.9 3.6 %collective-permute-start.29 = (bf16[32,1024]{1,0:T(8,128)(2,1)S(1)}, bf16[32,1024]{1,0:T(8,128)(2,1)S(1)}, u32[]{:S(2)}, u32[]{:S(2)}) collective-permute-start(bf16[32,1024]{1,0:T(8,128)(2,1)S(1)} %get-tuple-element.42), channel_id=1, source_target_pairs={{0,20},{1,21},{2,22},{3,23},{4,16},{5,17},{6,18},{7,19},{8,28},{9,... | collective-permute-start | bytes 196616 | tf_op jit(solution)/shard_map/ppermute | solution.py:23
  77.7 2.4 %collective-permute-start.21 = (bf16[32,2048]{1,0:T(8,128)(2,1)S(1)}, bf16[32,2048]{1,0:T(8,128)(2,1)S(1)}, u32[]{:S(2)}, u32[]{:S(2)}) collective-permute-start(bf16[32,2048]{1,0:T(8,128)(2,1)S(1)} %get-tuple-element.38), channel_id=1, source_target_pairs={{0,12},{1,13},{2,14},{3,15},{4,8},{5,9},{6,10},{7,11},{8,4},{9,5},... | collective-permute-start | bytes 393224 | tf_op jit(solution)/shard_map/ppermute | solution.py:23
  85.3 3.0 %collective-permute-done.30.refs_1_ = bf16[64,1024]{1,0:T(8,128)(2,1)S(1)} collective-permute-done((bf16[64,1024]{1,0:T(8,128)(2,1)S(1)}, bf16[64,1024]{1,0:T(8,128)(2,1)S(1)}, u32[]{:S(2)}, u32[]{:S(2)}) %collective-permute-start.30) | collective-permute-done | bytes 131104 | tf_op jit(solution)/shard_map/ppermute | solution.py:23
  88.3 2.0 %shard_map.189 = (bf16[64,2048]{1,0:T(8,128)(2,1)S(1)}, bf16[64,2048]{1,0:T(8,128)(2,1)S(1)}) custom-call(bf16[64,1024]{1,0:T(8,128)(2,1)S(1)} %constant_dynamic-update-slice_fusion.6.refs_0_, bf16[64,1024]{1,0:T(8,128)(2,1)S(1)} %collective-permute-done.39.refs_1_, bf16[64,1024]{1,0:T(8,128)(2,1)S(1)} %collective-permute-done.40.refs_2_, ...), custom_call_target="tpu_custom_call" | custom-call | flops 805306368 | tf_op jit(solution)/shard_map/pallas_call | solution.py:74
  91.0 2.0 %shard_map.188 = (bf16[64,2048]{1,0:T(8,128)(2,1)S(1)}, bf16[64,2048]{1,0:T(8,128)(2,1)S(1)}) custom-call(bf16[64,1024]{1,0:T(8,128)(2,1)S(1)} %constant_dynamic-update-slice_fusion.4.refs_0_, bf16[64,1024]{1,0:T(8,128)(2,1)S(1)} %collective-permute-done.30.refs_1_, bf16[64,1024]{1,0:T(8,128)(2,1)S(1)} %collective-permute-done.31.refs_2_, ...), custom_call_target="tpu_custom_call" | custom-call | flops 805306368 | tf_op jit(solution)/shard_map/pallas_call | solution.py:74
  95.3 2.0 %shard_map.187 = (bf16[128,2048]{1,0:T(8,128)(2,1)S(1)}, bf16[128,2048]{1,0:T(8,128)(2,1)S(1)}) custom-call(bf16[128,2048]{1,0:T(8,128)(2,1)S(1)} %constant_dynamic-update-slice_fusion.refs_0_, bf16[128,2048]{1,0:T(8,128)(2,1)S(1)} %collective-permute-done.22.refs_1_, f32[1,4096]{1,0:T(1,128)S(1)} %bitcast.11, bf16[1,4096,512]{2,1,0:T(8,128)(2,1)S(1)} %copy-done, ...), custom_call_target="tpu_custom_call" | custom-call | flops 1610612736 | tf_op jit(solution)/shard_map/pallas_call | solution.py:74
  101.0 1.9 %collective-permute-start.44 = (bf16[32,1024]{1,0:T(8,128)(2,1)S(1)}, bf16[32,1024]{1,0:T(8,128)(2,1)S(1)}, u32[]{:S(2)}, u32[]{:S(2)}) collective-permute-start(bf16[32,1024]{1,0:T(8,128)(2,1)S(1)} %get-tuple-element.70), channel_id=1, source_target_pairs={{0,24},{1,25},{2,26},{3,27},{4,28},{5,29},{6,30},{7,31},{8,16},{9,... | collective-permute-start | bytes 196616 | tf_op jit(solution)/shard_map/ppermute | solution.py:23
  104.0 5.1 %collective-permute-done.24 = bf16[128,1024]{1,0:T(8,128)(2,1)S(1)} collective-permute-done((bf16[128,1024]{1,0:T(8,128)(2,1)S(1)}, bf16[128,1024]{1,0:T(8,128)(2,1)S(1)}, u32[]{:S(2)}, u32[]{:S(2)}) %collective-permute-start.24) | collective-permute-done | bytes 262176 | tf_op jit(solution)/shard_map/ppermute | solution.py:23
  110.8 3.0 %collective-permute-start.36 = (bf16[32,1024]{1,0:T(8,128)(2,1)S(1)}, bf16[32,1024]{1,0:T(8,128)(2,1)S(1)}, u32[]{:S(2)}, u32[]{:S(2)}) collective-permute-start(bf16[32,1024]{1,0:T(8,128)(2,1)S(1)} %get-tuple-element.71), channel_id=1, source_target_pairs={{0,20},{1,21},{2,22},{3,23},{4,16},{5,17},{6,18},{7,19},{8,28},{9,... | collective-permute-start | bytes 196616 | tf_op jit(solution)/shard_map/ppermute | solution.py:23
  113.7 2.4 %collective-permute-start.45 = (bf16[32,1024]{1,0:T(8,128)(2,1)S(1)}, bf16[32,1024]{1,0:T(8,128)(2,1)S(1)}, u32[]{:S(2)}, u32[]{:S(2)}) collective-permute-start(bf16[32,1024]{1,0:T(8,128)(2,1)S(1)} %get-tuple-element.69), channel_id=1, source_target_pairs={{0,28},{1,29},{2,30},{3,31},{4,24},{5,25},{6,26},{7,27},{8,20},{9,... | collective-permute-start | bytes 196616 | tf_op jit(solution)/shard_map/ppermute | solution.py:23
  116.2 4.9 %collective-permute-done.26 = bf16[32,1024]{1,0:T(8,128)(2,1)S(1)} collective-permute-done((bf16[32,1024]{1,0:T(8,128)(2,1)S(1)}, bf16[32,1024]{1,0:T(8,128)(2,1)S(1)}, u32[]{:S(2)}, u32[]{:S(2)}) %collective-permute-start.26) | collective-permute-done | bytes 65568 | tf_op jit(solution)/shard_map/ppermute | solution.py:23
  121.5 4.8 %collective-permute-done.27 = bf16[32,1024]{1,0:T(8,128)(2,1)S(1)} collective-permute-done((bf16[32,1024]{1,0:T(8,128)(2,1)S(1)}, bf16[32,1024]{1,0:T(8,128)(2,1)S(1)}, u32[]{:S(2)}, u32[]{:S(2)}) %collective-permute-start.27) | collective-permute-done | bytes 65568 | tf_op jit(solution)/shard_map/ppermute | solution.py:23
  (160 shorter events, 47.9 us)
Async XLA Ops:
  1.7 7.3 %collective-permute-start = (bf16[64,512]{1,0:T(8,128)(2,1)S(1)}, bf16[64,512]{1,0:T(8,128)(2,1)S(1)}, u32[]{:S(2)}, u32[]{:S(2)}) collective-permute-start(bf16[64,512]{1,0:T(8,128)(2,1)S(1)} %get-tuple-element.56), channel_id=1, source_target_pairs={{0,0},{1,5},{2,2},{3,7},{4,4},{5,1},{6,6},{7,3},{8,8},{9,13},{10,1... | collective-permute-start | bytes 196616 | tf_op jit(solution)/shard_map/ppermute | solution.py:23
  6.4 7.9 %collective-permute-start.2 = (bf16[64,512]{1,0:T(8,128)(2,1)S(1)}, bf16[64,512]{1,0:T(8,128)(2,1)S(1)}, u32[]{:S(2)}, u32[]{:S(2)}) collective-permute-start(bf16[64,512]{1,0:T(8,128)(2,1)S(1)} %get-tuple-element.54), channel_id=1, source_target_pairs={{0,20},{1,17},{2,22},{3,19},{4,16},{5,21},{6,18},{7,23},{8,28},{9,... | collective-permute-start | bytes 196616 | tf_op jit(solution)/shard_map/ppermute | solution.py:23
  20.8 9.2 %collective-permute-start.14 = (bf16[256,512]{1,0:T(8,128)(2,1)S(1)}, bf16[256,512]{1,0:T(8,128)(2,1)S(1)}, u32[]{:S(2)}, u32[]{:S(2)}) collective-permute-start(bf16[256,512]{1,0:T(8,128)(2,1)S(1)} %convolution_convert_fusion), channel_id=1, source_target_pairs={{0,8},{1,9},{2,10},{3,11},{4,12},{5,13},{6,14},{7,15},{8,0},{9,1},... | collective-permute-start | bytes 786440 | tf_op jit(solution)/shard_map/ppermute | solution.py:23
  22.2 12.9 %collective-permute-start.11 = (bf16[256,512]{1,0:T(8,128)(2,1)S(1)}, bf16[256,512]{1,0:T(8,128)(2,1)S(1)}, u32[]{:S(2)}, u32[]{:S(2)}) collective-permute-start(bf16[256,512]{1,0:T(8,128)(2,1)S(1)} %convolution_convert_fusion.2), channel_id=1, source_target_pairs={{0,8},{1,9},{2,10},{3,11},{4,12},{5,13},{6,14},{7,15},{8,0},{9,1},... | collective-permute-start | bytes 786440 | tf_op jit(solution)/shard_map/ppermute | solution.py:23
  23.6 12.6 %collective-permute-start.8 = (bf16[256,512]{1,0:T(8,128)(2,1)S(1)}, bf16[256,512]{1,0:T(8,128)(2,1)S(1)}, u32[]{:S(2)}, u32[]{:S(2)}) collective-permute-start(bf16[256,512]{1,0:T(8,128)(2,1)S(1)} %convolution_convert_fusion.4), channel_id=1, source_target_pairs={{0,4},{1,5},{2,6},{3,7},{4,0},{5,1},{6,2},{7,3},{8,12},{9,13},{10,... | collective-permute-start | bytes 786440 | tf_op jit(solution)/shard_map/ppermute | solution.py:23
  25.0 13.5 %collective-permute-start.5 = (bf16[256,512]{1,0:T(8,128)(2,1)S(1)}, bf16[256,512]{1,0:T(8,128)(2,1)S(1)}, u32[]{:S(2)}, u32[]{:S(2)}) collective-permute-start(bf16[256,512]{1,0:T(8,128)(2,1)S(1)} %convolution_convert_fusion.6), channel_id=1, source_target_pairs={{0,4},{1,5},{2,6},{3,7},{4,0},{5,1},{6,2},{7,3},{8,12},{9,13},{10,... | collective-permute-start | bytes 786440 | tf_op jit(solution)/shard_map/ppermute | solution.py:23
  30.1 11.2 %collective-permute-start.15 = (bf16[128,512]{1,0:T(8,128)(2,1)S(1)}, bf16[128,512]{1,0:T(8,128)(2,1)S(1)}, u32[]{:S(2)}, u32[]{:S(2)}) collective-permute-start(bf16[128,512]{1,0:T(8,128)(2,1)S(1)} %add_convert_fusion.7), channel_id=1, source_target_pairs={{0,4},{1,5},{2,6},{3,7},{4,0},{5,1},{6,2},{7,3},{8,12},{9,13},{10,... | collective-permute-start | bytes 393224 | tf_op jit(solution)/shard_map/ppermute | solution.py:23
  35.1 8.3 %collective-permute-start.12 = (bf16[128,512]{1,0:T(8,128)(2,1)S(1)}, bf16[128,512]{1,0:T(8,128)(2,1)S(1)}, u32[]{:S(2)}, u32[]{:S(2)}) collective-permute-start(bf16[128,512]{1,0:T(8,128)(2,1)S(1)} %add_convert_fusion.8), channel_id=1, source_target_pairs={{0,4},{1,5},{2,6},{3,7},{4,0},{5,1},{6,2},{7,3},{8,12},{9,13},{10,... | collective-permute-start | bytes 393224 | tf_op jit(solution)/shard_map/ppermute | solution.py:23
  36.3 8.6 %collective-permute-start.9 = (bf16[128,512]{1,0:T(8,128)(2,1)S(1)}, bf16[128,512]{1,0:T(8,128)(2,1)S(1)}, u32[]{:S(2)}, u32[]{:S(2)}) collective-permute-start(bf16[128,512]{1,0:T(8,128)(2,1)S(1)} %add_convert_fusion.9), channel_id=1, source_target_pairs={{0,8},{1,9},{2,10},{3,11},{4,12},{5,13},{6,14},{7,15},{8,0},{9,1},... | collective-permute-start | bytes 393224 | tf_op jit(solution)/shard_map/ppermute | solution.py:23
  38.5 8.0 %collective-permute-start.6 = (bf16[128,512]{1,0:T(8,128)(2,1)S(1)}, bf16[128,512]{1,0:T(8,128)(2,1)S(1)}, u32[]{:S(2)}, u32[]{:S(2)}) collective-permute-start(bf16[128,512]{1,0:T(8,128)(2,1)S(1)} %add_convert_fusion.10), channel_id=1, source_target_pairs={{0,8},{1,9},{2,10},{3,11},{4,12},{5,13},{6,14},{7,15},{8,0},{9,1},... | collective-permute-start | bytes 393224 | tf_op jit(solution)/shard_map/ppermute | solution.py:23
  41.3 9.9 %collective-permute-start.16 = (bf16[64,512]{1,0:T(8,128)(2,1)S(1)}, bf16[64,512]{1,0:T(8,128)(2,1)S(1)}, u32[]{:S(2)}, u32[]{:S(2)}) collective-permute-start(bf16[64,512]{1,0:T(8,128)(2,1)S(1)} %add_convert_fusion.11), channel_id=1, source_target_pairs={{0,16},{1,17},{2,18},{3,19},{4,20},{5,21},{6,22},{7,23},{8,24},{9,... | collective-permute-start | bytes 196616 | tf_op jit(solution)/shard_map/ppermute | solution.py:23
  43.4 9.9 %collective-permute-start.13 = (bf16[64,512]{1,0:T(8,128)(2,1)S(1)}, bf16[64,512]{1,0:T(8,128)(2,1)S(1)}, u32[]{:S(2)}, u32[]{:S(2)}) collective-permute-start(bf16[64,512]{1,0:T(8,128)(2,1)S(1)} %add_convert_fusion.12), channel_id=1, source_target_pairs={{0,16},{1,17},{2,18},{3,19},{4,20},{5,21},{6,22},{7,23},{8,24},{9,... | collective-permute-start | bytes 196616 | tf_op jit(solution)/shard_map/ppermute | solution.py:23
  44.9 9.7 %collective-permute-start.10 = (bf16[64,512]{1,0:T(8,128)(2,1)S(1)}, bf16[64,512]{1,0:T(8,128)(2,1)S(1)}, u32[]{:S(2)}, u32[]{:S(2)}) collective-permute-start(bf16[64,512]{1,0:T(8,128)(2,1)S(1)} %add_convert_fusion.13), channel_id=1, source_target_pairs={{0,16},{1,17},{2,18},{3,19},{4,20},{5,21},{6,22},{7,23},{8,24},{9,... | collective-permute-start | bytes 196616 | tf_op jit(solution)/shard_map/ppermute | solution.py:23
  46.6 8.7 %collective-permute-start.7 = (bf16[64,512]{1,0:T(8,128)(2,1)S(1)}, bf16[64,512]{1,0:T(8,128)(2,1)S(1)}, u32[]{:S(2)}, u32[]{:S(2)}) collective-permute-start(bf16[64,512]{1,0:T(8,128)(2,1)S(1)} %add_convert_fusion.14), channel_id=1, source_target_pairs={{0,16},{1,17},{2,18},{3,19},{4,20},{5,21},{6,22},{7,23},{8,24},{9,... | collective-permute-start | bytes 196616 | tf_op jit(solution)/shard_map/ppermute | solution.py:23
  59.6 8.4 %collective-permute-start.18 = (bf16[64,2048]{1,0:T(8,128)(2,1)S(1)}, bf16[64,2048]{1,0:T(8,128)(2,1)S(1)}, u32[]{:S(2)}, u32[]{:S(2)}) collective-permute-start(bf16[64,2048]{1,0:T(8,128)(2,1)S(1)} %add_convert_fusion.4.refs_1_), channel_id=1, source_target_pairs={{0,2},{1,3},{2,0},{3,1},{4,6},{5,7},{6,4},{7,5},{8,10},{9,11},{10,... | collective-permute-start | bytes 786440 | tf_op jit(solution)/shard_map/ppermute | solution.py:23
  68.7 8.6 %collective-permute-start.37 = (bf16[32,1024]{1,0:T(8,128)(2,1)S(1)}, bf16[32,1024]{1,0:T(8,128)(2,1)S(1)}, u32[]{:S(2)}, u32[]{:S(2)}) collective-permute-start(bf16[32,1024]{1,0:T(8,128)(2,1)S(1)} %get-tuple-element.45), channel_id=1, source_target_pairs={{0,24},{1,25},{2,26},{3,27},{4,28},{5,29},{6,30},{7,31},{8,16},{9,... | collective-permute-start | bytes 196616 | tf_op jit(solution)/shard_map/ppermute | solution.py:23
  72.9 9.4 %collective-permute-start.29 = (bf16[32,1024]{1,0:T(8,128)(2,1)S(1)}, bf16[32,1024]{1,0:T(8,128)(2,1)S(1)}, u32[]{:S(2)}, u32[]{:S(2)}) collective-permute-start(bf16[32,1024]{1,0:T(8,128)(2,1)S(1)} %get-tuple-element.42), channel_id=1, source_target_pairs={{0,20},{1,21},{2,22},{3,23},{4,16},{5,17},{6,18},{7,19},{8,28},{9,... | collective-permute-start | bytes 196616 | tf_op jit(solution)/shard_map/ppermute | solution.py:23
  77.4 7.4 %collective-permute-start.20 = (bf16[32,2048]{1,0:T(8,128)(2,1)S(1)}, bf16[32,2048]{1,0:T(8,128)(2,1)S(1)}, u32[]{:S(2)}, u32[]{:S(2)}) collective-permute-start(bf16[32,2048]{1,0:T(8,128)(2,1)S(1)} %get-tuple-element.37), channel_id=1, source_target_pairs={{0,8},{1,9},{2,10},{3,11},{4,12},{5,13},{6,14},{7,15},{8,0},{9,1},... | collective-permute-start | bytes 393224 | tf_op jit(solution)/shard_map/ppermute | solution.py:23
  77.7 13.3 %collective-permute-start.21 = (bf16[32,2048]{1,0:T(8,128)(2,1)S(1)}, bf16[32,2048]{1,0:T(8,128)(2,1)S(1)}, u32[]{:S(2)}, u32[]{:S(2)}) collective-permute-start(bf16[32,2048]{1,0:T(8,128)(2,1)S(1)} %get-tuple-element.38), channel_id=1, source_target_pairs={{0,12},{1,13},{2,14},{3,15},{4,8},{5,9},{6,10},{7,11},{8,4},{9,5},... | collective-permute-start | bytes 393224 | tf_op jit(solution)/shard_map/ppermute | solution.py:23
  99.5 9.6 %collective-permute-start.24 = (bf16[128,1024]{1,0:T(8,128)(2,1)S(1)}, bf16[128,1024]{1,0:T(8,128)(2,1)S(1)}, u32[]{:S(2)}, u32[]{:S(2)}) collective-permute-start(bf16[128,1024]{1,0:T(8,128)(2,1)S(1)} %slice.205), channel_id=1, source_target_pairs={{0,2},{1,3},{2,0},{3,1},{4,6},{5,7},{6,4},{7,5},{8,10},{9,11},{10,... | collective-permute-start | bytes 786440 | tf_op jit(solution)/shard_map/ppermute | solution.py:23
  101.0 25.3 %collective-permute-start.44 = (bf16[32,1024]{1,0:T(8,128)(2,1)S(1)}, bf16[32,1024]{1,0:T(8,128)(2,1)S(1)}, u32[]{:S(2)}, u32[]{:S(2)}) collective-permute-start(bf16[32,1024]{1,0:T(8,128)(2,1)S(1)} %get-tuple-element.70), channel_id=1, source_target_pairs={{0,24},{1,25},{2,26},{3,27},{4,28},{5,29},{6,30},{7,31},{8,16},{9,... | collective-permute-start | bytes 196616 | tf_op jit(solution)/shard_map/ppermute | solution.py:23
  110.4 15.9 %collective-permute-start.35 = (bf16[32,1024]{1,0:T(8,128)(2,1)S(1)}, bf16[32,1024]{1,0:T(8,128)(2,1)S(1)}, u32[]{:S(2)}, u32[]{:S(2)}) collective-permute-start(bf16[32,1024]{1,0:T(8,128)(2,1)S(1)} %get-tuple-element.72), channel_id=1, source_target_pairs={{0,16},{1,17},{2,18},{3,19},{4,20},{5,21},{6,22},{7,23},{8,24},{9,... | collective-permute-start | bytes 196616 | tf_op jit(solution)/shard_map/ppermute | solution.py:23
  110.8 15.5 %collective-permute-start.36 = (bf16[32,1024]{1,0:T(8,128)(2,1)S(1)}, bf16[32,1024]{1,0:T(8,128)(2,1)S(1)}, u32[]{:S(2)}, u32[]{:S(2)}) collective-permute-start(bf16[32,1024]{1,0:T(8,128)(2,1)S(1)} %get-tuple-element.71), channel_id=1, source_target_pairs={{0,20},{1,21},{2,22},{3,23},{4,16},{5,17},{6,18},{7,19},{8,28},{9,... | collective-permute-start | bytes 196616 | tf_op jit(solution)/shard_map/ppermute | solution.py:23
  113.7 12.6 %collective-permute-start.45 = (bf16[32,1024]{1,0:T(8,128)(2,1)S(1)}, bf16[32,1024]{1,0:T(8,128)(2,1)S(1)}, u32[]{:S(2)}, u32[]{:S(2)}) collective-permute-start(bf16[32,1024]{1,0:T(8,128)(2,1)S(1)} %get-tuple-element.69), channel_id=1, source_target_pairs={{0,28},{1,29},{2,30},{3,31},{4,24},{5,25},{6,26},{7,27},{8,20},{9,... | collective-permute-start | bytes 196616 | tf_op jit(solution)/shard_map/ppermute | solution.py:23
  (39 other events, 589.9 us)
